TPU v7x, 32 devices: a whole 2x2x4 slice. The times are simulated.
32 devices in a mesh: ep: 8 (over z, y), tp: 4 (over x, core).
Axes of the slice: x: 2, y: 2, z: 4, core: 2. Of those that a mesh axis runs over, the one named last changes fastest.
Arguments:
- hidden: bfloat16 [256, 2048], P('ep')
- norm_gains: float32 [4, 2048], replicated, may hold values from 0.1 to 1.9
- w_query: bfloat16 [2048, 1024], P(None, 'tp'), may hold values from -0.125 to 0.125
- w_key: bfloat16 [2048, 1024], P(None, 'tp'), may hold values from -0.125 to 0.125
- w_value: bfloat16 [2048, 1024], P(None, 'tp'), may hold values from -0.125 to 0.125
- w_outgate: bfloat16 [2048, 1024], P(None, 'tp'), may hold values from -0.125 to 0.125
- w_input_gate: bfloat16 [2048, 8], replicated, may hold values from -0.125 to 0.125
- w_forget_gate: bfloat16 [2048, 8], replicated, may hold values from -0.125 to 0.125
- forget_bias: float32 [8], replicated, may hold values from -1 to 4
- w_mix_out: bfloat16 [1024, 2048], P('tp')
- state_matrix: float32 [256, 8, 128, 128], P('ep', 'tp'), may hold values from -0.6 to 0.6
- state_norm: float32 [256, 8, 128], P('ep', 'tp'), may hold values from -0.6 to 0.6
- state_max: float32 [256, 8], P('ep', 'tp'), may hold values from -4 to 4
- routes: int32 [256, 2], P('ep'), may hold values from 0 to 7, all different within a row; in each aligned block of 32 rows (0 to 31, 32 to 63, ...) at most 16 rows name the same one
- route_scores: float32 [256, 2], P('ep'), may hold values from 0.1 to 1
- expert_gate: bfloat16 [8, 2048, 3584], P('ep', None, 'tp'), may hold values from -0.125 to 0.125
- expert_up: bfloat16 [8, 2048, 3584], P('ep', None, 'tp'), may hold values from -0.125 to 0.125
- expert_down: bfloat16 [8, 3584, 2048], P('ep', 'tp')
- dense_gate: bfloat16 [2048, 5632], P('tp', 'ep'), may hold values from -0.125 to 0.125
- dense_up: bfloat16 [2048, 5632], P('tp', 'ep'), may hold values from -0.125 to 0.125
- dense_down: bfloat16 [5632, 2048], P('ep', 'tp')
- dense_mix: float32 [2048], replicated, may hold values from -0.25 to 0.25
Outputs:
- new_hidden: bfloat16 [256, 2048], P('ep', 'tp')
- new_matrix: float32 [256, 8, 128, 128], P('ep', 'tp')
- new_norm: float32 [256, 8, 128], P('ep', 'tp')
- new_max: float32 [256, 8], P('ep', 'tp')
Inputs may be any that keep to these rules, and one draw needn't show every extreme that they name: `routes`: each row names 2 different experts. Among the rows of one index of ep (an aligned block of 32 rows) no expert is named by more than 16 rows, and in every draw some expert is named by exactly 16 rows of some block.
All inputs are finite; a program needn't handle non-finite values.
Results may differ from a plain program's by a relative error of at most 0.02.
Values may be sent and summed in bfloat16 or wider, within the bound.
A program may use at most 128 MiB of HBM per device.

v0:
```python
import functools

import jax
import jax.numpy as jnp
from jax import lax
from jax.experimental import pallas as pl
from jax.experimental.pallas import tpu as pltpu
from jax.sharding import PartitionSpec as P

EPS = 1e-06


def front_kernel(
    hidden_ref,
    gains_ref,
    in_ref,
    forget_ref,
    bias_ref,
    norm_ref,
    max_ref,
    wq_hbm,
    wk_hbm,
    wv_hbm,
    wo_hbm,
    wm_hbm,
    state_hbm,
    terms_ref,
    matrix_hbm,
    new_norm_ref,
    new_max_ref,
    wq,
    wk,
    wv,
    wo,
    wm,
    state,
    numer,
    w_sem,
    in_sem,
    out_sem,
):
    tp = lax.axis_index("tp")
    f32, bf16 = jnp.float32, jnp.bfloat16
    seqs = hidden_ref.shape[0]
    heads, head = state.shape[1], state.shape[2]
    chunks = in_sem.shape[0]
    step = seqs // chunks
    loads = []
    for i, (src, dst) in enumerate(((wk_hbm, wk), (wq_hbm, wq), (wv_hbm, wv), (wo_hbm, wo))):
        loads.append(pltpu.make_async_copy(src, dst, w_sem.at[i]))
        loads[i].start()
    fetches = []
    for c in range(chunks):
        rows = pl.ds(c * step, step)
        fetches.append(pltpu.make_async_copy(state_hbm.at[rows], state.at[rows], in_sem.at[c]))
        fetches[c].start()
    loads.append(pltpu.make_async_copy(wm_hbm, wm, w_sem.at[4]))
    loads[4].start()

    start = hidden_ref[...].astype(f32)
    scale = lax.rsqrt(jnp.mean(start * start, axis=1, keepdims=True) + EPS)
    normed = (start * scale * gains_ref[0:1, :]).astype(bf16)
    last = (((1,), (1,)), ((), ()))
    in_all = lax.dot_general(normed, in_ref[...], last, preferred_element_type=f32)
    forget_all = lax.dot_general(normed, forget_ref[...], last, preferred_element_type=f32)
    forget_all = forget_all + bias_ref[...]
    forget_all = jnp.minimum(forget_all, 0.0) - jnp.log(1.0 + jnp.exp(-jnp.abs(forget_all)))
    column = lax.broadcasted_iota(jnp.int32, in_all.shape, 1)
    here = lax.broadcasted_iota(jnp.int32, (seqs, seqs), 0)
    there = lax.broadcasted_iota(jnp.int32, (seqs, seqs), 1)
    projected = []
    for i, weight in enumerate((wk, wq, wv)):
        loads[i].wait()
        product = jnp.dot(normed, weight[...], preferred_element_type=f32)
        projected.append(product.astype(bf16).astype(f32))
    keys, query, values = projected
    pieces = []
    for h in range(heads):
        span = slice(h * head, (h + 1) * head)
        pieces.extend((keys[:, span], query[:, span]))
    turned = jnp.concatenate(pieces, axis=0).T
    keeps = []
    adds = []
    bounds = []
    for h in range(heads):
        span = slice(h * head, (h + 1) * head)
        mine = column == tp * heads + h
        in_gate = jnp.sum(jnp.where(mine, in_all, 0.0), axis=1, keepdims=True)
        log_forget = jnp.sum(jnp.where(mine, forget_all, 0.0), axis=1, keepdims=True)
        before = jnp.sum(jnp.where(here == there, max_ref[h : h + 1, :], 0.0), axis=1, keepdims=True)
        carried = log_forget + before
        new_max = jnp.maximum(carried, in_gate)
        keep = jnp.exp(carried - new_max)
        write = jnp.exp(in_gate - new_max) * head ** (-0.5)
        new_max_ref[h : h + 1, :] = jnp.sum(
            jnp.where(here == there, new_max, 0.0), axis=0, keepdims=True
        )
        new_norm = keep * norm_ref[:, h, :] + write * keys[:, span]
        new_norm_ref[:, h, :] = new_norm
        denom = jnp.sum(query[:, span] * new_norm, axis=1, keepdims=True)
        bounds.append(jnp.maximum(jnp.abs(denom), jnp.exp(-new_max)))
        keeps.append(jnp.broadcast_to(keep, (seqs, head)))
        adds.append(write * values[:, span])
    stores = []
    for c in range(chunks):
        fetches[c].wait()
        for s in range(c * step, (c + 1) * step):
            for h in range(heads):
                at = 2 * h * seqs + s
                key_col = turned[:, at : at + 1]
                query_col = turned[:, at + seqs : at + seqs + 1]
                new = keeps[h][s : s + 1, :] * state[s, h] + key_col * adds[h][s : s + 1, :]
                state[s, h] = new
                numer[h, s : s + 1, :] = jnp.sum(query_col * new, axis=0, keepdims=True)
        rows = pl.ds(c * step, step)
        stores.append(pltpu.make_async_copy(state.at[rows], matrix_hbm.at[rows], out_sem.at[c]))
        stores[c].start()
    loads[3].wait()
    gate = jnp.dot(normed, wo[...], preferred_element_type=f32).astype(bf16).astype(f32)
    mixed = []
    for h in range(heads):
        span = slice(h * head, (h + 1) * head)
        mixed.append((jax.nn.sigmoid(gate[:, span]) * (numer[h] / bounds[h])).astype(bf16))
    mixed = jnp.concatenate(mixed, axis=1)
    loads[4].wait()
    part = terms_ref.shape[2]
    for t in range(terms_ref.shape[0]):
        terms_ref[t] = jnp.dot(
            mixed, wm[:, t * part : (t + 1) * part], preferred_element_type=f32
        ).astype(bf16)
    for store in stores:
        store.wait()


def front(hidden, norm_gains, gate_weights, forget_bias, state_norm, state_max, weights, state_matrix):
    tp_count = lax.axis_size("tp")
    seqs, width = hidden.shape
    heads, head = state_matrix.shape[1], state_matrix.shape[2]
    f32, bf16 = jnp.float32, jnp.bfloat16
    chunks = 4
    vmem = pl.BlockSpec(memory_space=pltpu.VMEM)
    hbm = pl.BlockSpec(memory_space=pl.ANY)
    terms, matrix, norm, top = pl.pallas_call(
        front_kernel,
        out_shape=(
            jax.ShapeDtypeStruct((tp_count, seqs, width // tp_count), bf16),
            jax.ShapeDtypeStruct(state_matrix.shape, f32),
            jax.ShapeDtypeStruct(state_norm.shape, f32),
            jax.ShapeDtypeStruct((heads, seqs), f32),
        ),
        in_specs=[vmem] * 7 + [hbm] * 6,
        out_specs=(vmem, hbm, vmem, vmem),
        scratch_shapes=[pltpu.VMEM(weight.shape, bf16) for weight in weights]
        + [
            pltpu.VMEM(state_matrix.shape, f32),
            pltpu.VMEM((heads, seqs, head), f32),
            pltpu.SemaphoreType.DMA((5,)),
            pltpu.SemaphoreType.DMA((chunks,)),
            pltpu.SemaphoreType.DMA((chunks,)),
        ],
        compiler_params=pltpu.CompilerParams(vmem_limit_bytes=67043328),
        name="front",
    )(
        hidden,
        norm_gains,
        gate_weights[0].T,
        gate_weights[1].T,
        forget_bias.reshape(1, -1),
        state_norm,
        state_max.T,
        *weights,
        state_matrix,
    )
    return terms, matrix, norm, top.T


MESH = pl.DeviceIdType.MESH


def tail_kernel(
    tp_count,
    ep_count,
    capacity,
    terms_ref,
    hidden_ref,
    gains_ref,
    mix_ref,
    routes_ref,
    scores_ref,
    eg_hbm,
    eu_hbm,
    ed_hbm,
    dg_hbm,
    du_hbm,
    dd_hbm,
    out_ref,
    eg,
    eu,
    ed,
    dg,
    du,
    dd,
    br_recv,
    st_send,
    st_recv,
    fs_send,
    fs_recv,
    code_send,
    code_recv,
    rows_in,
    xin,
    pre_send,
    pre_one,
    pre_mid,
    pre_two,
    hid,
    down_send,
    down_recv,
    eo_send,
    eo_one,
    eo_mid,
    eo_two,
    sum_send,
    returned,
    w_sem,
    tp_send,
    tp_recv,
    ep_send,
    ep_recv,
):
    tp = lax.axis_index("tp")
    ep = lax.axis_index("ep")
    seqs, width = hidden_ref.shape
    part = width // tp_count
    rows_all = ep_count * seqs
    rows_tp = rows_all // tp_count
    first = pl.multiple_of(tp * part, part)
    f32, bf16 = jnp.float32, jnp.bfloat16

    loads = []
    for i, (src, dst) in enumerate(
        ((dg_hbm, dg), (du_hbm, du), (eg_hbm.at[0], eg), (eu_hbm.at[0], eu), (dd_hbm, dd), (ed_hbm.at[0], ed))
    ):
        load = pltpu.make_async_copy(src, dst, w_sem.at[i])
        load.start()
        loads.append(load)

    barrier = pltpu.get_barrier_semaphore()
    for d in range(1, tp_count):
        pl.semaphore_signal(
            barrier, inc=1, device_id={"tp": lax.rem(tp + d, tp_count)}, device_id_type=MESH
        )
    for d in range(1, ep_count):
        pl.semaphore_signal(
            barrier, inc=1, device_id={"ep": lax.rem(ep + d, ep_count)}, device_id_type=MESH
        )
    pl.semaphore_wait(barrier, tp_count - 1 + ep_count - 1)

    def tp_copies(phase, src_of, dst):
        made = []
        for d in range(1, tp_count):
            peer = lax.rem(tp + d, tp_count)
            copy = pltpu.make_async_remote_copy(
                src_ref=src_of(peer),
                dst_ref=dst,
                send_sem=tp_send.at[phase, d - 1],
                recv_sem=tp_recv.at[phase, d - 1],
                device_id={"tp": peer},
                device_id_type=MESH,
            )
            copy.start()
            made.append(copy)
        return made

    groups = tp_count // 2
    parity = lax.rem(tp, 2)
    group = tp // 2
    pair = tp + 1 - 2 * parity

    def one_copy(phase, i, src, dst, peer):
        copy = pltpu.make_async_remote_copy(
            src_ref=src,
            dst_ref=dst,
            send_sem=tp_send.at[phase, i],
            recv_sem=tp_recv.at[phase, i],
            device_id={"tp": peer},
            device_id_type=MESH,
        )
        copy.start()
        return copy

    def ahead(d):
        return lax.rem(group + d, groups) * 2 + parity

    def behind(d):
        return lax.rem(group + groups - d, groups) * 2 + parity

    def gather_start(phase, at):
        made = [one_copy(phase, d - 1, at(tp), at(tp), ahead(d)) for d in range(1, groups)]
        made.append(one_copy(phase, groups - 1, at(tp), at(tp), pair))
        return made

    def gather_relay(phase, at, made):
        for d in range(1, groups):
            made[d - 1].wait_recv()
            made.append(one_copy(phase, groups - 1 + d, at(behind(d)), at(behind(d)), pair))

    def scatter_pair(phase, at, one):
        return [
            one_copy(phase, j, at(j * 2 + 1 - parity), one.at[j], pair) for j in range(groups)
        ]

    def scatter_cross(phase, at, one, mid, two, made):
        arrive(made)
        for d in range(1, groups):
            j = lax.rem(group + d, groups)
            mid[j] = (at(ahead(d))[...].astype(f32) + one[j].astype(f32)).astype(bf16)
            made.append(one_copy(phase, groups + d - 1, mid.at[j], two.at[group], ahead(d)))

    def scatter_sum(at, one, two, made):
        total = at(tp)[...].astype(f32) + one[group].astype(f32)
        for d in range(1, groups):
            made[groups + d - 1].wait_recv()
            total = total + two[lax.rem(group + groups - d, groups)].astype(f32)
        return total

    def ep_copies(phase, src_of, dst):
        made = []
        for d in range(1, ep_count):
            peer = lax.rem(ep + d, ep_count)
            copy = pltpu.make_async_remote_copy(
                src_ref=src_of(peer),
                dst_ref=dst,
                send_sem=ep_send.at[phase, d - 1],
                recv_sem=ep_recv.at[phase, d - 1],
                device_id={"ep": peer},
                device_id_type=MESH,
            )
            copy.start()
            made.append(copy)
        return made

    def arrive(copies):
        for copy in copies:
            copy.wait_recv()

    def left(copies):
        for copy in copies:
            copy.wait_send()

    def from_tp(d):
        return lax.rem(tp + tp_count - d, tp_count)

    def from_ep(d):
        return lax.rem(ep + ep_count - d, ep_count)

    def columns(peer):
        return pl.ds(pl.multiple_of(peer * part, part), part)

    branch_copies = tp_copies(0, lambda peer: terms_ref.at[peer], br_recv.at[tp])
    top = routes_ref.shape[0]
    experts = code_send.shape[0]
    name = lax.broadcasted_iota(jnp.int32, (experts, seqs), 0)
    hits = [routes_ref[k : k + 1, :] == name for k in range(top)]
    named = hits[0]
    for k in range(1, top):
        named = jnp.logical_or(named, hits[k])
    named = jnp.where(named, 1.0, 0.0)
    here = lax.broadcasted_iota(jnp.int32, (seqs, seqs), 0)
    there = lax.broadcasted_iota(jnp.int32, (seqs, seqs), 1)
    before = jnp.where(here < there, 1.0, 0.0).astype(bf16)
    rank = jnp.dot(named.astype(bf16), before, preferred_element_type=f32) + 1.0
    code = (named * rank).astype(bf16)
    from_row = lax.broadcasted_iota(jnp.int32, (seqs, rows_all), 0)
    to_row = lax.broadcasted_iota(jnp.int32, (seqs, rows_all), 1)
    spread = jnp.where(from_row + ep * seqs == to_row, 1.0, 0.0).astype(bf16)
    code_send[...] = jnp.dot(code, spread, preferred_element_type=f32)
    code_copies = ep_copies(0, lambda peer: code_send, code_recv.at[ep])
    slots = ep_count * capacity
    owner = lax.broadcasted_iota(jnp.int32, (slots, experts), 0) // capacity
    of_expert = lax.broadcasted_iota(jnp.int32, (slots, experts), 1)
    widen = jnp.where(owner == of_expert, 1.0, 0.0).astype(bf16)
    row_slot = lax.broadcasted_iota(jnp.int32, (slots, seqs), 0)
    row_wanted = (lax.rem(row_slot, capacity) + 1).astype(f32)
    combines = []
    shares = []
    score_sum = scores_ref[0:1, :]
    for k in range(1, top):
        score_sum = score_sum + scores_ref[k : k + 1, :]
    for k in range(top):
        code_k = jnp.where(hits[k], rank, 0.0).astype(bf16)
        wide = jnp.dot(widen, code_k, preferred_element_type=f32)
        combines.append(jnp.where(wide == row_wanted, 1.0, 0.0).astype(bf16))
        share = scores_ref[k : k + 1, :] / score_sum
        shares.append(jnp.sum(jnp.where(here == there, share, 0.0), axis=1, keepdims=True))
    start_part = hidden_ref[:, pl.ds(first, part)].astype(f32)
    gain_one = gains_ref[1:2, pl.ds(first, part)]
    gain_two = gains_ref[2:3, pl.ds(first, part)]
    gain_three = gains_ref[3:4, pl.ds(first, part)]
    mix_weight = gain_two * mix_ref[:, pl.ds(first, part)]
    start_sq = jnp.sum(start_part * start_part, axis=1, keepdims=True)
    start_dot = jnp.sum(start_part * mix_weight, axis=1, keepdims=True)
    branch = terms_ref[tp].astype(f32)
    arrive(branch_copies)
    for d in range(1, tp_count):
        branch = branch + br_recv[from_tp(d)].astype(f32)
    branch = branch.astype(bf16).astype(f32)
    lifted = gain_one * branch
    sums = (
        jnp.sum(branch * branch, axis=1, keepdims=True),
        start_sq,
        jnp.sum(start_part * lifted, axis=1, keepdims=True),
        jnp.sum(lifted * lifted, axis=1, keepdims=True),
        start_dot,
        jnp.sum(lifted * mix_weight, axis=1, keepdims=True),
    )
    lane = lax.broadcasted_iota(jnp.int32, (seqs, 128), 1)
    packed = jnp.zeros((seqs, 128), f32)
    for i, value in enumerate(sums):
        packed = packed + jnp.where(lane == i, value, 0.0)
    st_send[...] = packed
    stat_copies = tp_copies(1, lambda peer: st_send, st_recv.at[tp])
    arrive(stat_copies)
    for d in range(1, tp_count):
        packed = packed + st_recv[from_tp(d)]
    branch_sq, start_sq, cross_sum, lifted_sq, start_dot, lifted_dot = (
        packed[:, i : i + 1] for i in range(6)
    )
    branch_scale = lax.rsqrt(branch_sq / width + EPS)
    residual_f = start_part + lifted * branch_scale
    resid_sq = start_sq + 2.0 * branch_scale * cross_sum + branch_scale * branch_scale * lifted_sq
    gate_dot = start_dot + branch_scale * lifted_dot
    scale_two = lax.rsqrt(resid_sq / width + EPS)
    mix_gate = jax.nn.sigmoid(scale_two * gate_dot)
    residual = residual_f.astype(bf16).astype(f32)
    normed = (residual_f * scale_two * gain_two).astype(bf16)
    my_rows = pl.ds(pl.multiple_of(ep * seqs, seqs), seqs)
    rows_in[my_rows, :] = normed
    row_copies = ep_copies(1, lambda peer: rows_in.at[my_rows], rows_in.at[my_rows])

    arrive(code_copies)
    codes = code_send[...]
    for d in range(1, ep_count):
        codes = codes + code_recv[from_ep(d)]
    expert = lax.broadcasted_iota(jnp.int32, codes.shape, 0)
    mine = jnp.sum(jnp.where(expert == ep, codes, 0.0), axis=0, keepdims=True)
    slot = lax.broadcasted_iota(jnp.int32, (slots, rows_all), 0)
    token = lax.broadcasted_iota(jnp.int32, (slots, rows_all), 1)
    wanted = (lax.rem(slot, capacity) + 1).astype(f32)
    placing = jnp.where(
        jnp.logical_and(slot // capacity == token // seqs, mine == wanted), 1.0, 0.0
    ).astype(bf16)

    arrive(row_copies)
    rows = rows_in[...]
    xin[tp] = jnp.dot(placing, rows, preferred_element_type=f32).astype(bf16)
    def block_rows(peer):
        return pl.ds(pl.multiple_of(peer * rows_tp, rows_tp), rows_tp)

    def xin_at(i):
        return xin.at[i]

    def pre_at(i):
        return pre_send.at[:, block_rows(i)]

    def hid_at(i):
        return hid.at[block_rows(i)]

    def eo_at(i):
        return eo_send.at[i]

    expert_copies = gather_start(2, xin_at)

    loads[0].wait()
    loads[1].wait()
    last = (((1,), (1,)), ((), ()))
    pre_send[0] = lax.dot_general(rows, dg[...], last, preferred_element_type=f32).astype(bf16)
    pre_send[1] = lax.dot_general(rows, du[...], last, preferred_element_type=f32).astype(bf16)
    pre_copies = scatter_pair(3, pre_at, pre_one)

    loads[2].wait()
    loads[3].wait()
    gate_pre = jnp.dot(xin[tp], eg[columns(tp), :], preferred_element_type=f32)
    up_pre = jnp.dot(xin[tp], eu[columns(tp), :], preferred_element_type=f32)
    scatter_cross(3, pre_at, pre_one, pre_mid, pre_two, pre_copies)
    expert_copies[groups - 1].wait_recv()
    gate_pre = gate_pre + jnp.dot(xin[pair], eg[columns(pair), :], preferred_element_type=f32)
    up_pre = up_pre + jnp.dot(xin[pair], eu[columns(pair), :], preferred_element_type=f32)
    gather_relay(2, xin_at, expert_copies)
    for d in range(1, groups):
        source = behind(d)
        gate_pre = gate_pre + jnp.dot(xin[source], eg[columns(source), :], preferred_element_type=f32)
        up_pre = up_pre + jnp.dot(xin[source], eu[columns(source), :], preferred_element_type=f32)
    for d in range(1, groups):
        expert_copies[groups - 1 + d].wait_recv()
        source = behind(d) + 1 - 2 * parity
        gate_pre = gate_pre + jnp.dot(xin[source], eg[columns(source), :], preferred_element_type=f32)
        up_pre = up_pre + jnp.dot(xin[source], eu[columns(source), :], preferred_element_type=f32)
    hidden_units = (jax.nn.silu(gate_pre) * up_pre).astype(bf16)

    pre = scatter_sum(pre_at, pre_one, pre_two, pre_copies)
    hid[block_rows(tp), :] = (jax.nn.silu(pre[0]) * pre[1]).astype(bf16)
    hid_copies = gather_start(4, hid_at)

    loads[5].wait()
    for j in range(groups):
        t = j * 2 + 1 - parity
        eo_send[t] = jnp.dot(hidden_units, ed[:, columns(t)], preferred_element_type=f32).astype(bf16)
    eo_copies = scatter_pair(5, eo_at, eo_one)
    for j in range(groups):
        t = j * 2 + parity
        eo_send[t] = jnp.dot(hidden_units, ed[:, columns(t)], preferred_element_type=f32).astype(bf16)
    scatter_cross(5, eo_at, eo_one, eo_mid, eo_two, eo_copies)
    gather_relay(4, hid_at, hid_copies)
    for copy in hid_copies[groups - 1 :]:
        copy.wait_recv()
    loads[4].wait()
    down_send[...] = jnp.dot(hid[...], dd[...], preferred_element_type=f32).astype(bf16)

    def seq_rows(peer):
        return pl.ds(pl.multiple_of(peer * seqs, seqs), seqs)

    down_copies = ep_copies(2, lambda peer: down_send.at[seq_rows(peer)], down_recv.at[ep])

    total = scatter_sum(eo_at, eo_one, eo_two, eo_copies)
    sum_send[...] = total.astype(bf16)

    def slot_rows(peer):
        return pl.ds(pl.multiple_of(peer * capacity, capacity), capacity)

    back_copies = ep_copies(3, lambda peer: sum_send.at[slot_rows(peer)], returned.at[slot_rows(ep)])
    returned[slot_rows(ep), :] = sum_send[slot_rows(ep), :]

    arrive(down_copies)
    dense_out = down_send[seq_rows(ep), :].astype(f32)
    for d in range(1, ep_count):
        dense_out = dense_out + down_recv[from_ep(d)].astype(f32)
    ffn = mix_gate * dense_out
    arrive(back_copies)
    first_dims = (((0,), (0,)), ((), ()))
    for k in range(top):
        picked = lax.dot_general(combines[k], returned[...], first_dims, preferred_element_type=f32)
        ffn = ffn + shares[k] * picked
    squares = jnp.where(lane == 0, jnp.sum(ffn * ffn, axis=1, keepdims=True), 0.0)
    fs_send[...] = squares
    final_copies = tp_copies(6, lambda peer: fs_send, fs_recv.at[tp])
    scaled = gain_three * ffn
    arrive(final_copies)
    for d in range(1, tp_count):
        squares = squares + fs_recv[from_tp(d)]
    out_ref[...] = (residual + scaled * lax.rsqrt(squares[:, 0:1] / width + EPS)).astype(bf16)
    for copies in (
        branch_copies,
        code_copies,
        stat_copies,
        row_copies,
        expert_copies,
        pre_copies,
        hid_copies,
        eo_copies,
        down_copies,
        back_copies,
        final_copies,
    ):
        left(copies)


def tail(
    terms, hidden, norm_gains, dense_mix, routes, route_scores, weights
):
    tp_count = lax.axis_size("tp")
    ep_count = lax.axis_size("ep")
    seqs, width = hidden.shape
    part = width // tp_count
    expert_gate, expert_up, expert_down, dense_gate, dense_up, dense_down = weights
    units = expert_gate.shape[2]
    dense_gate, dense_up = dense_gate.T, dense_up.T
    dense_units = dense_gate.shape[0]
    top = routes.shape[1]
    experts = ep_count * expert_gate.shape[0]
    limit = 2 * seqs * top // ep_count
    capacity = -(-limit // 16) * 16
    rows_all = ep_count * seqs
    rows_tp = rows_all // tp_count
    groups = tp_count // 2
    f32, bf16 = jnp.float32, jnp.bfloat16
    vmem = pl.BlockSpec(memory_space=pltpu.VMEM)
    hbm = pl.BlockSpec(memory_space=pl.ANY)
    slots = ep_count * capacity
    return pl.pallas_call(
        functools.partial(tail_kernel, tp_count, ep_count, capacity),
        out_shape=jax.ShapeDtypeStruct((seqs, part), bf16),
        in_specs=[vmem] * 6 + [hbm] * 6,
        out_specs=vmem,
        scratch_shapes=[
            pltpu.VMEM((width, units), bf16),
            pltpu.VMEM((width, units), bf16),
            pltpu.VMEM((units, width), bf16),
            pltpu.VMEM(dense_gate.shape, bf16),
            pltpu.VMEM(dense_up.shape, bf16),
            pltpu.VMEM(dense_down.shape, bf16),
            pltpu.VMEM((tp_count, seqs, part), bf16),
            pltpu.VMEM((seqs, 128), f32),
            pltpu.VMEM((tp_count, seqs, 128), f32),
            pltpu.VMEM((seqs, 128), f32),
            pltpu.VMEM((tp_count, seqs, 128), f32),
            pltpu.VMEM((experts, rows_all), f32),
            pltpu.VMEM((ep_count, experts, rows_all), f32),
            pltpu.VMEM((rows_all, part), bf16),
            pltpu.VMEM((tp_count, slots, part), bf16),
            pltpu.VMEM((2, rows_all, dense_units), bf16),
            pltpu.VMEM((groups, 2, rows_tp, dense_units), bf16),
            pltpu.VMEM((groups, 2, rows_tp, dense_units), bf16),
            pltpu.VMEM((groups, 2, rows_tp, dense_units), bf16),
            pltpu.VMEM((rows_all, dense_units), bf16),
            pltpu.VMEM((rows_all, part), bf16),
            pltpu.VMEM((ep_count, seqs, part), bf16),
            pltpu.VMEM((tp_count, slots, part), bf16),
            pltpu.VMEM((groups, slots, part), bf16),
            pltpu.VMEM((groups, slots, part), bf16),
            pltpu.VMEM((groups, slots, part), bf16),
            pltpu.VMEM((slots, part), bf16),
            pltpu.VMEM((slots, part), bf16),
            pltpu.SemaphoreType.DMA((6,)),
            pltpu.SemaphoreType.DMA((7, tp_count - 1)),
            pltpu.SemaphoreType.DMA((7, tp_count - 1)),
            pltpu.SemaphoreType.DMA((4, ep_count - 1)),
            pltpu.SemaphoreType.DMA((4, ep_count - 1)),
        ],
        compiler_params=pltpu.CompilerParams(
            collective_id=0, has_side_effects=True, vmem_limit_bytes=67043328
        ),
        name="tail",
    )(
        terms,
        hidden,
        norm_gains,
        dense_mix.reshape(1, width),
        routes.T,
        route_scores.T,
        expert_gate,
        expert_up,
        expert_down,
        dense_gate,
        dense_up,
        dense_down,
    )


def local(
    hidden,
    norm_gains,
    w_query,
    w_key,
    w_value,
    w_outgate,
    w_input_gate,
    w_forget_gate,
    forget_bias,
    w_mix_out,
    state_matrix,
    state_norm,
    state_max,
    routes,
    route_scores,
    expert_gate,
    expert_up,
    expert_down,
    dense_gate,
    dense_up,
    dense_down,
    dense_mix,
):
    terms, new_matrix, new_norm, new_max = front(
        hidden,
        norm_gains,
        (w_input_gate, w_forget_gate),
        forget_bias,
        state_norm,
        state_max,
        (w_query, w_key, w_value, w_outgate, w_mix_out),
        state_matrix,
    )
    new_hidden = tail(
        terms,
        hidden,
        norm_gains,
        dense_mix,
        routes,
        route_scores,
        (expert_gate, expert_up, expert_down, dense_gate, dense_up, dense_down),
    )
    return (new_hidden, new_matrix, new_norm, new_max)


def solution(mesh):
    placed = (
        P("ep", None),
        P(),
        P(None, "tp"),
        P(None, "tp"),
        P(None, "tp"),
        P(None, "tp"),
        P(),
        P(),
        P(),
        P("tp", None),
        P("ep", "tp", None, None),
        P("ep", "tp", None),
        P("ep", "tp"),
        P("ep", None),
        P("ep", None),
        P("ep", None, "tp"),
        P("ep", None, "tp"),
        P("ep", "tp", None),
        P("tp", "ep"),
        P("tp", "ep"),
        P("ep", "tp"),
        P(),
    )
    return jax.shard_map(
        local,
        mesh=mesh,
        in_specs=placed,
        out_specs=(P("ep", "tp"), P("ep", "tp", None, None), P("ep", "tp", None), P("ep", "tp")),
        check_vma=False,
    )
```

profile of v0, /device:TPU:0, one launch (start us, length us, event | category | flops | bytes accessed | tf_op | source)
XLA Modules:
  0.0 57.6 jit_solution(3262366959568186824)
XLA Ops:
  0.6 8.0 %front.1 = (bf16[4,32,512]{2,1,0:T(8,128)(2,1)}, f32[32,2,128,128]{3,2,1,0:T(8,128)}, f32[32,2,128]{2,1,0:T(2,128)}, f32[2,32]{1,0:T(2,128)}) custom-call(bf16[32,2048]{1,0:T(8,128)(2,1)} %hidden_ref.3, f32[4,2048]{1,0:T(4,128)} %gains_ref.3, bf16[8,2048]{1,0:T(8,128)(2,1)} %bitcast.12, bf16[8,2048]{1,0:T(8,128)(2,1)} %bitcast.13, f32[1,8]{1,0:T(1,128)} %bitcast.18, ...), custom_call_target="tpu_custom_call" | custom-call | tf_op jit(solution)/shard_map/front/pallas_call | solution.py:143
  8.6 47.5 %tail.1 = bf16[32,512]{1,0:T(8,128)(2,1)} custom-call(bf16[4,32,512]{2,1,0:T(8,128)(2,1)} %get-tuple-element.8.terms_ref, bf16[32,2048]{1,0:T(8,128)(2,1)} %hidden_ref.3, f32[4,2048]{1,0:T(4,128)} %gains_ref.3, f32[1,2048]{1,0:T(1,128)} %bitcast.14, s32[2,32]{1,0:T(2,128)} %bitcast.16, f32[2,32]{1,0:T(2,128)} %bitcast.17, bf16[1,2048,896]{2,1,0:T(8,128)(2,1)} %eg_hbm.1, ...), custom_call_target="tpu_custom_call" | custom-call | tf_op jit(solution)/shard_map/tail/pallas_call | solution.py:590
  56.2 1.4 %copy.27 = bf16[32,512]{1,0:T(8,128)(2,1)} copy(bf16[32,512]{1,0:T(8,128)(2,1)} %tail.1) | data formatting | bytes 65536
where the time goes:
time: 57.8 us; the launch traced here: 57.6 us
  Pallas kernels  55.5 us (96%)
  local copies, waits for them, and re-layouts  1.38 us (2%)
  between operations  0.65 us (1%)
    pallas_call x1, Pallas kernels, tail(): pl.pallas_call(functools.partial(tail_kernel, tp_count, ep_count, capacit...  47.5 us
    pallas_call x1, Pallas kernels, front(): pl.pallas_call(front_kernel, out_shape=(jax.ShapeDtypeStruct((tp_count, s...  7.98 us
    unnamed x1, local copies, waits for them, and re-layouts  1.38 us

commit v1 on v0

v1 whole, which is shorter than its diff:
```python
import functools

import jax
import jax.numpy as jnp
from jax import lax
from jax.experimental import pallas as pl
from jax.experimental.pallas import tpu as pltpu
from jax.sharding import PartitionSpec as P

EPS = 1e-06


def front_kernel(
    hidden_ref,
    gains_ref,
    in_ref,
    forget_ref,
    bias_ref,
    norm_ref,
    max_ref,
    wq_hbm,
    wk_hbm,
    wv_hbm,
    wo_hbm,
    wm_hbm,
    state_hbm,
    terms_ref,
    matrix_hbm,
    new_norm_ref,
    new_max_ref,
    wq,
    wk,
    wv,
    wo,
    wm,
    state,
    numer,
    w_sem,
    in_sem,
    out_sem,
):
    tp = lax.axis_index("tp")
    f32, bf16 = jnp.float32, jnp.bfloat16
    seqs = hidden_ref.shape[0]
    heads, head = state.shape[1], state.shape[2]
    chunks = in_sem.shape[0]
    step = seqs // chunks
    loads = []
    for i, (src, dst) in enumerate(((wk_hbm, wk), (wq_hbm, wq), (wv_hbm, wv), (wo_hbm, wo))):
        loads.append(pltpu.make_async_copy(src, dst, w_sem.at[i]))
        loads[i].start()
    fetches = []
    for c in range(chunks):
        rows = pl.ds(c * step, step)
        fetches.append(pltpu.make_async_copy(state_hbm.at[rows], state.at[rows], in_sem.at[c]))
        fetches[c].start()
    loads.append(pltpu.make_async_copy(wm_hbm, wm, w_sem.at[4]))
    loads[4].start()

    start = hidden_ref[...].astype(f32)
    scale = lax.rsqrt(jnp.mean(start * start, axis=1, keepdims=True) + EPS)
    normed = (start * scale * gains_ref[0:1, :]).astype(bf16)
    last = (((1,), (1,)), ((), ()))
    in_all = lax.dot_general(normed, in_ref[...], last, preferred_element_type=f32)
    forget_all = lax.dot_general(normed, forget_ref[...], last, preferred_element_type=f32)
    forget_all = forget_all + bias_ref[...]
    forget_all = jnp.minimum(forget_all, 0.0) - jnp.log(1.0 + jnp.exp(-jnp.abs(forget_all)))
    column = lax.broadcasted_iota(jnp.int32, in_all.shape, 1)
    here = lax.broadcasted_iota(jnp.int32, (seqs, seqs), 0)
    there = lax.broadcasted_iota(jnp.int32, (seqs, seqs), 1)
    projected = []
    for i, weight in enumerate((wk, wq, wv)):
        loads[i].wait()
        product = jnp.dot(normed, weight[...], preferred_element_type=f32)
        projected.append(product.astype(bf16).astype(f32))
    keys, query, values = projected
    pieces = []
    for h in range(heads):
        span = slice(h * head, (h + 1) * head)
        pieces.extend((keys[:, span], query[:, span]))
    turned = jnp.concatenate(pieces, axis=0).T
    keeps = []
    adds = []
    bounds = []
    for h in range(heads):
        span = slice(h * head, (h + 1) * head)
        mine = column == tp * heads + h
        in_gate = jnp.sum(jnp.where(mine, in_all, 0.0), axis=1, keepdims=True)
        log_forget = jnp.sum(jnp.where(mine, forget_all, 0.0), axis=1, keepdims=True)
        before = jnp.sum(jnp.where(here == there, max_ref[h : h + 1, :], 0.0), axis=1, keepdims=True)
        carried = log_forget + before
        new_max = jnp.maximum(carried, in_gate)
        keep = jnp.exp(carried - new_max)
        write = jnp.exp(in_gate - new_max) * head ** (-0.5)
        new_max_ref[h : h + 1, :] = jnp.sum(
            jnp.where(here == there, new_max, 0.0), axis=0, keepdims=True
        )
        new_norm = keep * norm_ref[:, h, :] + write * keys[:, span]
        new_norm_ref[:, h, :] = new_norm
        denom = jnp.sum(query[:, span] * new_norm, axis=1, keepdims=True)
        bounds.append(jnp.maximum(jnp.abs(denom), jnp.exp(-new_max)))
        keeps.append(jnp.broadcast_to(keep, (seqs, head)))
        adds.append(write * values[:, span])
    stores = []
    for c in range(chunks):
        fetches[c].wait()
        for s in range(c * step, (c + 1) * step):
            for h in range(heads):
                at = 2 * h * seqs + s
                key_col = turned[:, at : at + 1]
                query_col = turned[:, at + seqs : at + seqs + 1]
                new = keeps[h][s : s + 1, :] * state[s, h] + key_col * adds[h][s : s + 1, :]
                state[s, h] = new
                numer[h, s : s + 1, :] = jnp.sum(query_col * new, axis=0, keepdims=True)
        rows = pl.ds(c * step, step)
        stores.append(pltpu.make_async_copy(state.at[rows], matrix_hbm.at[rows], out_sem.at[c]))
        stores[c].start()
    loads[3].wait()
    gate = jnp.dot(normed, wo[...], preferred_element_type=f32).astype(bf16).astype(f32)
    mixed = []
    for h in range(heads):
        span = slice(h * head, (h + 1) * head)
        mixed.append((jax.nn.sigmoid(gate[:, span]) * (numer[h] / bounds[h])).astype(bf16))
    mixed = jnp.concatenate(mixed, axis=1)
    loads[4].wait()
    part = terms_ref.shape[2]
    for t in range(terms_ref.shape[0]):
        terms_ref[t] = jnp.dot(
            mixed, wm[:, t * part : (t + 1) * part], preferred_element_type=f32
        ).astype(bf16)
    for store in stores:
        store.wait()


def front(hidden, norm_gains, gate_weights, forget_bias, state_norm, state_max, weights, state_matrix):
    tp_count = lax.axis_size("tp")
    seqs, width = hidden.shape
    heads, head = state_matrix.shape[1], state_matrix.shape[2]
    f32, bf16 = jnp.float32, jnp.bfloat16
    chunks = 4
    vmem = pl.BlockSpec(memory_space=pltpu.VMEM)
    hbm = pl.BlockSpec(memory_space=pl.ANY)
    terms, matrix, norm, top = pl.pallas_call(
        front_kernel,
        out_shape=(
            jax.ShapeDtypeStruct((tp_count, seqs, width // tp_count), bf16),
            jax.ShapeDtypeStruct(state_matrix.shape, f32),
            jax.ShapeDtypeStruct(state_norm.shape, f32),
            jax.ShapeDtypeStruct((heads, seqs), f32),
        ),
        in_specs=[vmem] * 7 + [hbm] * 6,
        out_specs=(vmem, hbm, vmem, vmem),
        scratch_shapes=[pltpu.VMEM(weight.shape, bf16) for weight in weights]
        + [
            pltpu.VMEM(state_matrix.shape, f32),
            pltpu.VMEM((heads, seqs, head), f32),
            pltpu.SemaphoreType.DMA((5,)),
            pltpu.SemaphoreType.DMA((chunks,)),
            pltpu.SemaphoreType.DMA((chunks,)),
        ],
        compiler_params=pltpu.CompilerParams(vmem_limit_bytes=67043328),
        name="front",
    )(
        hidden,
        norm_gains,
        gate_weights[0].T,
        gate_weights[1].T,
        forget_bias.reshape(1, -1),
        state_norm,
        state_max.T,
        *weights,
        state_matrix,
    )
    return terms, matrix, norm, top.T


MESH = pl.DeviceIdType.MESH


def tail_kernel(
    tp_count,
    ep_count,
    capacity,
    chunks,
    terms_hbm,
    hidden_hbm,
    gains_hbm,
    mix_hbm,
    routes_hbm,
    scores_hbm,
    eg_hbm,
    eu_hbm,
    ed_hbm,
    dg_hbm,
    du_hbm,
    dd_hbm,
    out_ref,
    terms,
    start_in,
    gains,
    mix,
    routes,
    scores,
    eg,
    eu,
    ed,
    dg,
    du,
    dd,
    br_recv,
    st_send,
    st_recv,
    fs_send,
    fs_recv,
    info_send,
    info_recv,
    mg_send,
    mg_recv,
    rows_in,
    xin,
    pre_send,
    pre_one,
    pre_mid,
    pre_two,
    hid,
    dense_out,
    eo_send,
    eo_one,
    eo_mid,
    eo_two,
    c_send,
    c_recv,
    s_sem,
    w_sem,
    tp_send,
    tp_recv,
    ep_send,
    ep_recv,
):
    tp = lax.axis_index("tp")
    ep = lax.axis_index("ep")
    seqs, part = start_in.shape
    width = part * tp_count
    per = ep_count // chunks
    chunk_rows = per * seqs
    chunk_slots = per * capacity
    quarter = chunk_rows // tp_count
    halves = 2
    half_chunks = chunks // halves
    half_slots = half_chunks * chunk_slots
    half_rows = half_chunks * chunk_rows
    first = pl.multiple_of(tp * part, part)
    f32, bf16 = jnp.float32, jnp.bfloat16

    own = pl.ds(first, part)
    smalls = []
    for i, (src, dst) in enumerate(
        (
            (terms_hbm, terms),
            (hidden_hbm.at[:, own], start_in),
            (gains_hbm.at[:, own], gains),
            (mix_hbm.at[:, own], mix),
            (routes_hbm, routes),
            (scores_hbm, scores),
        )
    ):
        load = pltpu.make_async_copy(src, dst, s_sem.at[i])
        load.start()
        smalls.append(load)

    barrier = pltpu.get_barrier_semaphore()
    for d in range(1, tp_count):
        pl.semaphore_signal(
            barrier, inc=1, device_id={"tp": lax.rem(tp + d, tp_count)}, device_id_type=MESH
        )
    for d in range(1, ep_count):
        pl.semaphore_signal(
            barrier, inc=1, device_id={"ep": lax.rem(ep + d, ep_count)}, device_id_type=MESH
        )

    loads = []
    for i, (src, dst) in enumerate(
        ((dg_hbm, dg), (du_hbm, du), (eg_hbm.at[0], eg), (eu_hbm.at[0], eu), (ed_hbm.at[0], ed), (dd_hbm, dd))
    ):
        load = pltpu.make_async_copy(src, dst, w_sem.at[i])
        load.start()
        loads.append(load)

    groups = tp_count // 2
    parity = lax.rem(tp, 2)
    group = tp // 2
    pair = tp + 1 - 2 * parity
    started = []
    tp_next = [0]
    ep_next = [0]

    def tp_copy(src, dst, peer):
        at = tp_next[0]
        tp_next[0] += 1
        copy = pltpu.make_async_remote_copy(
            src_ref=src,
            dst_ref=dst,
            send_sem=tp_send.at[at],
            recv_sem=tp_recv.at[at],
            device_id={"tp": peer},
            device_id_type=MESH,
        )
        copy.start()
        started.append(copy)
        return copy

    gray = [k ^ (k >> 1) for k in range(chunks)]
    order = [gray[k] * per + i for k in range(chunks) for i in range(per)]

    def partner(p):
        other = ep
        bit = 1
        while bit < ep_count:
            if order[p] & bit:
                other = other + bit * (1 - 2 * lax.rem(ep // bit, 2))
            bit *= 2
        return other

    def ep_copy(src, dst, p):
        at = ep_next[0]
        ep_next[0] += 1
        copy = pltpu.make_async_remote_copy(
            src_ref=src,
            dst_ref=dst,
            send_sem=ep_send.at[at],
            recv_sem=ep_recv.at[at],
            device_id={"ep": partner(p)},
            device_id_type=MESH,
        )
        copy.start()
        started.append(copy)
        return copy

    def tp_all(src_of, dst):
        made = []
        for d in range(1, tp_count):
            peer = lax.rem(tp + d, tp_count)
            made.append(tp_copy(src_of(peer), dst, peer))
        return made

    def ahead(d):
        return lax.rem(group + d, groups) * 2 + parity

    def behind(d):
        return lax.rem(group + groups - d, groups) * 2 + parity

    def gather_start(at):
        made = [tp_copy(at(tp), at(tp), ahead(d)) for d in range(1, groups)]
        made.append(tp_copy(at(tp), at(tp), pair))
        return made

    def gather_relay(at, made):
        for d in range(1, groups):
            made[d - 1].wait_recv()
            made.append(tp_copy(at(behind(d)), at(behind(d)), pair))

    def scatter_pair(at, one):
        return [tp_copy(at(j * 2 + 1 - parity), one(j), pair) for j in range(groups)]

    def scatter_cross(at, one, mid, two, made):
        arrive(made)
        for d in range(1, groups):
            j = lax.rem(group + d, groups)
            mid(j)[...] = (at(ahead(d))[...].astype(f32) + one(j)[...].astype(f32)).astype(bf16)
            made.append(tp_copy(mid(j), two(group), ahead(d)))

    def scatter_sum(at, one, two, made):
        total = at(tp)[...].astype(f32) + one(group)[...].astype(f32)
        for d in range(1, groups):
            made[groups + d - 1].wait_recv()
            total = total + two(lax.rem(group + groups - d, groups))[...].astype(f32)
        return total

    def arrive(copies):
        for copy in copies:
            copy.wait_recv()

    def from_tp(d):
        return lax.rem(tp + tp_count - d, tp_count)

    def columns(peer):
        return pl.ds(pl.multiple_of(peer * part, part), part)

    for ref in (st_send, fs_send, mg_send, info_send):
        ref[...] = jnp.zeros(ref.shape, f32)
    here = lax.broadcasted_iota(jnp.int32, (seqs, seqs), 0)
    there = lax.broadcasted_iota(jnp.int32, (seqs, seqs), 1)
    diagonal = here == there

    def to_row(column):
        return jnp.sum(jnp.where(diagonal, column, 0.0), axis=0, keepdims=True)

    def to_column(row):
        return jnp.sum(jnp.where(diagonal, row, 0.0), axis=1, keepdims=True)

    for load in smalls:
        load.wait()
    pl.semaphore_wait(barrier, tp_count - 1 + ep_count - 1)
    branch_copies = tp_all(lambda peer: terms.at[peer], br_recv.at[tp])

    top = routes.shape[0]
    experts = info_send.shape[1]
    name = lax.broadcasted_iota(jnp.int32, (experts, seqs), 0)
    hits = [routes[k : k + 1, :] == name for k in range(top)]
    named = hits[0]
    for k in range(1, top):
        named = jnp.logical_or(named, hits[k])
    named = jnp.where(named, 1.0, 0.0)
    before = jnp.where(here < there, 1.0, 0.0).astype(bf16)
    rank = jnp.dot(named.astype(bf16), before, preferred_element_type=f32) + 1.0
    score_sum = scores[0:1, :]
    for k in range(1, top):
        score_sum = score_sum + scores[k : k + 1, :]
    share = jnp.zeros((experts, seqs), f32)
    for k in range(top):
        share = share + jnp.where(hits[k], scores[k : k + 1, :] / score_sum, 0.0)
    info_send[0, :, 0:seqs] = named * rank
    info_send[1, :, 0:seqs] = share
    info_copies = [ep_copy(info_send, info_recv.at[p], p) for p in range(1, ep_count)]

    start_part = start_in[...].astype(f32)
    gain_one = gains[1:2, :]
    gain_two = gains[2:3, :]
    gain_three = gains[3:4, :]
    mix_weight = gain_two * mix[...]
    start_sq = jnp.sum(start_part * start_part, axis=1, keepdims=True)
    start_dot = jnp.sum(start_part * mix_weight, axis=1, keepdims=True)
    branch = terms[tp].astype(f32)
    arrive(branch_copies)
    for d in range(1, tp_count):
        branch = branch + br_recv[from_tp(d)].astype(f32)
    branch = branch.astype(bf16).astype(f32)
    lifted = gain_one * branch
    sums = (
        jnp.sum(branch * branch, axis=1, keepdims=True),
        start_sq,
        jnp.sum(start_part * lifted, axis=1, keepdims=True),
        jnp.sum(lifted * lifted, axis=1, keepdims=True),
        start_dot,
        jnp.sum(lifted * mix_weight, axis=1, keepdims=True),
    )
    for i, value in enumerate(sums):
        st_send[i : i + 1, 0:seqs] = to_row(value)
    stat_copies = tp_all(lambda peer: st_send, st_recv.at[tp])
    packed = st_send[...]
    arrive(stat_copies)
    for d in range(1, tp_count):
        packed = packed + st_recv[from_tp(d)]
    branch_sq, start_sq, cross_sum, lifted_sq, start_dot, lifted_dot = (
        packed[i : i + 1, 0:seqs] for i in range(6)
    )
    branch_scale = lax.rsqrt(branch_sq / width + EPS)
    resid_sq = start_sq + 2.0 * branch_scale * cross_sum + branch_scale * branch_scale * lifted_sq
    gate_dot = start_dot + branch_scale * lifted_dot
    scale_two = lax.rsqrt(resid_sq / width + EPS)
    mg_send[0:1, 0:seqs] = jax.nn.sigmoid(scale_two * gate_dot)
    residual_f = start_part + lifted * to_column(branch_scale)
    residual = residual_f.astype(bf16).astype(f32)
    rows_in[0] = (residual_f * to_column(scale_two) * gain_two).astype(bf16)
    row_copies = [ep_copy(rows_in.at[0], rows_in.at[p], p) for p in range(1, ep_count)]
    mg_copies = [ep_copy(mg_send, mg_recv.at[p], p) for p in range(1, ep_count)]

    mine = lax.broadcasted_iota(jnp.int32, (experts, seqs), 0) == ep
    wanted = (lax.broadcasted_iota(jnp.int32, (capacity, seqs), 0) + 1).astype(f32)
    placings = []
    shares = []

    def place(p):
        if p == 0:
            codes, portion = info_send[0], info_send[1]
        else:
            info_copies[p - 1].wait_recv()
            codes, portion = info_recv[p, 0], info_recv[p, 1]
        code = jnp.sum(jnp.where(mine, codes[:, 0:seqs], 0.0), axis=0, keepdims=True)
        placings.append(jnp.where(code == wanted, 1.0, 0.0).astype(bf16))
        shares.append(jnp.sum(jnp.where(mine, portion[:, 0:seqs], 0.0), axis=0, keepdims=True))

    def slots_of(p):
        return pl.ds(p * capacity, capacity)

    def xin_at(k):
        return lambda i: xin.at[i, pl.ds(k * chunk_slots, chunk_slots)]

    def pre_at(k):
        return lambda i: pre_send.at[k, i]

    def of(ref, k):
        return lambda j: ref.at[k, j]

    def hid_at(k):
        return lambda i: hid.at[k, i]

    def half_of(ref, h):
        return lambda i: ref.at[i, pl.ds(h * half_slots, half_slots)]

    last = (((1,), (1,)), ((), ()))
    xin_copies = []
    pre_copies = []
    hid_copies = []

    def chunk_in(k):
        for p in range(k * per, (k + 1) * per):
            place(p)
            if p > 0:
                row_copies[p - 1].wait_recv()
            xin[tp, slots_of(p)] = jnp.dot(
                placings[p], rows_in[p], preferred_element_type=f32
            ).astype(bf16)
        xin_copies.append(gather_start(xin_at(k)))
        if k == 0:
            loads[0].wait()
            loads[1].wait()
        rows = rows_in[k * per : (k + 1) * per].reshape(chunk_rows, part)
        for i, weight in enumerate((dg, du)):
            made = lax.dot_general(rows, weight[...], last, preferred_element_type=f32).astype(bf16)
            for t in range(tp_count):
                pre_send[k, t, i] = made[t * quarter : (t + 1) * quarter]
        pre_copies.append(scatter_pair(pre_at(k), of(pre_one, k)))

    def pre_cross(k):
        scatter_cross(pre_at(k), of(pre_one, k), of(pre_mid, k), of(pre_two, k), pre_copies[k])

    def pre_done(k):
        pre = scatter_sum(pre_at(k), of(pre_one, k), of(pre_two, k), pre_copies[k])
        hid[k, tp] = (jax.nn.silu(pre[0]) * pre[1]).astype(bf16)
        hid_copies.append(gather_start(hid_at(k)))

    def xin_relay(k):
        gather_relay(xin_at(k), xin_copies[k])

    def hid_relay(k):
        gather_relay(hid_at(k), hid_copies[k])

    sums_of = [None, None]

    def expert_in(source):
        for i, weight in enumerate((eg, eu)):
            made = jnp.dot(xin[source], weight[columns(source), :], preferred_element_type=f32)
            sums_of[i] = made if sums_of[i] is None else sums_of[i] + made

    for k in range(chunks):
        chunk_in(k)
        if k >= 1:
            pre_cross(k - 1)
        if k >= 2:
            xin_relay(k - 2)
    if chunks >= 2:
        xin_relay(chunks - 2)
    loads[2].wait()
    loads[3].wait()
    expert_in(tp)
    pre_cross(chunks - 1)
    pre_done(0)
    for k in range(chunks):
        xin_copies[k][groups - 1].wait_recv()
    expert_in(pair)
    xin_relay(chunks - 1)
    pre_done(1)
    for d in range(1, groups):
        expert_in(behind(d))
    pre_done(2)
    for d in range(1, groups):
        for k in range(chunks):
            xin_copies[k][groups - 1 + d].wait_recv()
        expert_in(behind(d) + 1 - 2 * parity)
    hidden_units = (jax.nn.silu(sums_of[0]) * sums_of[1]).astype(bf16)

    loads[4].wait()
    eo_copies = [None] * halves
    turn = list(range(halves))[::-1]

    def expert_down(h, t):
        eo_send[t, h * half_slots : (h + 1) * half_slots] = jnp.dot(
            hidden_units[h * half_slots : (h + 1) * half_slots],
            ed[:, columns(t)],
            preferred_element_type=f32,
        ).astype(bf16)

    for h in turn:
        for j in range(groups):
            expert_down(h, j * 2 + 1 - parity)
        eo_copies[h] = scatter_pair(half_of(eo_send, h), half_of(eo_one, h))
    for k in range(3, chunks):
        pre_done(k)
    for k in range(chunks - 1):
        hid_relay(k)
    for h in turn:
        for j in range(groups):
            expert_down(h, j * 2 + parity)
        scatter_cross(
            half_of(eo_send, h), half_of(eo_one, h), half_of(eo_mid, h), half_of(eo_two, h), eo_copies[h]
        )
    hid_relay(chunks - 1)
    loads[5].wait()
    c_copies = {}
    mixed = None
    for h in turn:
        for k in range(h * half_chunks, (h + 1) * half_chunks):
            arrive(hid_copies[k][groups - 1 :])
        units = hid.shape[3]
        dense_out[h * half_rows : (h + 1) * half_rows] = jnp.dot(
            hid[h * half_chunks : (h + 1) * half_chunks].reshape(half_rows, units),
            dd[...],
            preferred_element_type=f32,
        )
    first_dims = (((0,), (0,)), ((), ()))
    for h in turn:
        total = scatter_sum(half_of(eo_send, h), half_of(eo_one, h), half_of(eo_two, h), eo_copies[h])
        total = total.astype(bf16)
        for q in list(range(half_chunks * per))[::-1]:
            p = h * half_chunks * per + q
            picked = lax.dot_general(
                placings[p],
                total[q * capacity : (q + 1) * capacity],
                first_dims,
                preferred_element_type=f32,
            )
            if p == 0:
                gate = mg_send[0:1, 0:seqs]
            else:
                mg_copies[p - 1].wait_recv()
                gate = mg_recv[p, 0:1, 0:seqs]
            combined = (
                to_column(gate) * dense_out[p * seqs : (p + 1) * seqs] + to_column(shares[p]) * picked
            )
            if p == 0:
                mixed = combined
            else:
                c_send[p] = combined.astype(bf16)
                c_copies[p] = ep_copy(c_send.at[p], c_recv.at[p], p)
    ffn = mixed
    for p in range(1, ep_count):
        c_copies[p].wait_recv()
        ffn = ffn + c_recv[p].astype(f32)
    fs_send[0:1, 0:seqs] = to_row(jnp.sum(ffn * ffn, axis=1, keepdims=True))
    final_copies = tp_all(lambda peer: fs_send, fs_recv.at[tp])
    scaled = gain_three * ffn
    squares = fs_send[...]
    arrive(final_copies)
    for d in range(1, tp_count):
        squares = squares + fs_recv[from_tp(d)]
    scale = to_column(lax.rsqrt(squares[0:1, 0:seqs] / width + EPS))
    out_ref[...] = (residual + scaled * scale).astype(bf16)
    for copy in started:
        copy.wait_send()


def tail(
    terms, hidden, norm_gains, dense_mix, routes, route_scores, weights
):
    tp_count = lax.axis_size("tp")
    ep_count = lax.axis_size("ep")
    seqs, width = hidden.shape
    part = width // tp_count
    expert_gate, expert_up, expert_down, dense_gate, dense_up, dense_down = weights
    units = expert_gate.shape[2]
    dense_gate, dense_up = dense_gate.T, dense_up.T
    dense_units = dense_gate.shape[0]
    top = routes.shape[1]
    experts = ep_count * expert_gate.shape[0]
    limit = 2 * seqs * top // ep_count
    capacity = -(-limit // 16) * 16
    chunks = 4
    rows_all = ep_count * seqs
    quarter = rows_all // chunks // tp_count
    groups = tp_count // 2
    lanes = -(-seqs // 128) * 128
    f32, bf16 = jnp.float32, jnp.bfloat16
    vmem = pl.BlockSpec(memory_space=pltpu.VMEM)
    hbm = pl.BlockSpec(memory_space=pl.ANY)
    slots = ep_count * capacity
    tp_copies = 3 * (tp_count - 1) + (3 * chunks + 2) * (2 * groups - 1)
    ep_copies = 4 * (ep_count - 1)
    piece = pltpu.VMEM((chunks, groups, 2, quarter, dense_units), bf16)
    return pl.pallas_call(
        functools.partial(tail_kernel, tp_count, ep_count, capacity, chunks),
        out_shape=jax.ShapeDtypeStruct((seqs, part), bf16),
        in_specs=[hbm] * 12,
        out_specs=vmem,
        scratch_shapes=[
            pltpu.VMEM((tp_count, seqs, part), bf16),
            pltpu.VMEM((seqs, part), bf16),
            pltpu.VMEM((norm_gains.shape[0], part), f32),
            pltpu.VMEM((1, part), f32),
            pltpu.VMEM((top, seqs), jnp.int32),
            pltpu.VMEM((top, seqs), f32),
            pltpu.VMEM((width, units), bf16),
            pltpu.VMEM((width, units), bf16),
            pltpu.VMEM((units, width), bf16),
            pltpu.VMEM(dense_gate.shape, bf16),
            pltpu.VMEM(dense_up.shape, bf16),
            pltpu.VMEM(dense_down.shape, bf16),
            pltpu.VMEM((tp_count, seqs, part), bf16),
            pltpu.VMEM((8, lanes), f32),
            pltpu.VMEM((tp_count, 8, lanes), f32),
            pltpu.VMEM((1, lanes), f32),
            pltpu.VMEM((tp_count, 1, lanes), f32),
            pltpu.VMEM((2, experts, lanes), f32),
            pltpu.VMEM((ep_count, 2, experts, lanes), f32),
            pltpu.VMEM((1, lanes), f32),
            pltpu.VMEM((ep_count, 1, lanes), f32),
            pltpu.VMEM((ep_count, seqs, part), bf16),
            pltpu.VMEM((tp_count, slots, part), bf16),
            pltpu.VMEM((chunks, tp_count, 2, quarter, dense_units), bf16),
            piece,
            piece,
            piece,
            pltpu.VMEM((chunks, tp_count, quarter, dense_units), bf16),
            pltpu.VMEM((rows_all, part), f32),
            pltpu.VMEM((tp_count, slots, part), bf16),
            pltpu.VMEM((groups, slots, part), bf16),
            pltpu.VMEM((groups, slots, part), bf16),
            pltpu.VMEM((groups, slots, part), bf16),
            pltpu.VMEM((ep_count, seqs, part), bf16),
            pltpu.VMEM((ep_count, seqs, part), bf16),
            pltpu.SemaphoreType.DMA((6,)),
            pltpu.SemaphoreType.DMA((6,)),
            pltpu.SemaphoreType.DMA((tp_copies,)),
            pltpu.SemaphoreType.DMA((tp_copies,)),
            pltpu.SemaphoreType.DMA((ep_copies,)),
            pltpu.SemaphoreType.DMA((ep_copies,)),
        ],
        compiler_params=pltpu.CompilerParams(
            collective_id=0, has_side_effects=True, vmem_limit_bytes=67043328
        ),
        name="tail",
    )(
        terms,
        hidden,
        norm_gains,
        dense_mix.reshape(1, width),
        routes.T,
        route_scores.T,
        expert_gate,
        expert_up,
        expert_down,
        dense_gate,
        dense_up,
        dense_down,
    )


def local(
    hidden,
    norm_gains,
    w_query,
    w_key,
    w_value,
    w_outgate,
    w_input_gate,
    w_forget_gate,
    forget_bias,
    w_mix_out,
    state_matrix,
    state_norm,
    state_max,
    routes,
    route_scores,
    expert_gate,
    expert_up,
    expert_down,
    dense_gate,
    dense_up,
    dense_down,
    dense_mix,
):
    terms, new_matrix, new_norm, new_max = front(
        hidden,
        norm_gains,
        (w_input_gate, w_forget_gate),
        forget_bias,
        state_norm,
        state_max,
        (w_query, w_key, w_value, w_outgate, w_mix_out),
        state_matrix,
    )
    new_hidden = tail(
        terms,
        hidden,
        norm_gains,
        dense_mix,
        routes,
        route_scores,
        (expert_gate, expert_up, expert_down, dense_gate, dense_up, dense_down),
    )
    return (new_hidden, new_matrix, new_norm, new_max)


def solution(mesh):
    placed = (
        P("ep", None),
        P(),
        P(None, "tp"),
        P(None, "tp"),
        P(None, "tp"),
        P(None, "tp"),
        P(),
        P(),
        P(),
        P("tp", None),
        P("ep", "tp", None, None),
        P("ep", "tp", None),
        P("ep", "tp"),
        P("ep", None),
        P("ep", None),
        P("ep", None, "tp"),
        P("ep", None, "tp"),
        P("ep", "tp", None),
        P("tp", "ep"),
        P("tp", "ep"),
        P("ep", "tp"),
        P(),
    )
    return jax.shard_map(
        local,
        mesh=mesh,
        in_specs=placed,
        out_specs=(P("ep", "tp"), P("ep", "tp", None, None), P("ep", "tp", None), P("ep", "tp")),
        check_vma=False,
    )
```

time: 57.8 us -> 52.4 us (0.907)
  Pallas kernels: 55.5 us -> 50.2 us
    pallas_call x1, Pallas kernels: 47.5 us -> 42.2 us  [tail(): pl.pallas_call(functools.partial(tail_kernel, tp_count, ep_count, capacit...]
where the time goes in v1:
time: 52.4 us; the launch traced here: 52.2 us
  Pallas kernels  50.2 us (96%)
  local copies, waits for them, and re-layouts  1.38 us (3%)
  between operations  0.65 us (1%)
    pallas_call x1, Pallas kernels, tail(): pl.pallas_call(functools.partial(tail_kernel, tp_count, ep_count, capacit...  42.2 us
    pallas_call x1, Pallas kernels, front(): pl.pallas_call(front_kernel, out_shape=(jax.ShapeDtypeStruct((tp_count, s...  7.98 us
    unnamed x1, local copies, waits for them, and re-layouts  1.38 us

profile of v1, /device:TPU:0, one launch (start us, length us, event | category | flops | bytes accessed | tf_op | source)
XLA Modules:
  0.0 52.2 jit_solution(10979135505204624944)
XLA Ops:
  0.6 8.0 %front.1 = (bf16[4,32,512]{2,1,0:T(8,128)(2,1)}, f32[32,2,128,128]{3,2,1,0:T(8,128)}, f32[32,2,128]{2,1,0:T(2,128)}, f32[2,32]{1,0:T(2,128)}) custom-call(bf16[32,2048]{1,0:T(8,128)(2,1)} %hidden_hbm.1, f32[4,2048]{1,0:T(4,128)} %gains_hbm.1, bf16[8,2048]{1,0:T(8,128)(2,1)} %bitcast.12, bf16[8,2048]{1,0:T(8,128)(2,1)} %bitcast.13, f32[1,8]{1,0:T(1,128)} %bitcast.18, ...), custom_call_target="tpu_custom_call" | custom-call | tf_op jit(solution)/shard_map/front/pallas_call | solution.py:143
  8.6 42.2 %tail.1 = bf16[32,512]{1,0:T(8,128)(2,1)} custom-call(bf16[4,32,512]{2,1,0:T(8,128)(2,1)} %get-tuple-element.8.terms_hbm, bf16[32,2048]{1,0:T(8,128)(2,1)} %hidden_hbm.1, f32[4,2048]{1,0:T(4,128)} %gains_hbm.1, f32[1,2048]{1,0:T(1,128)} %bitcast.14, s32[2,32]{1,0:T(2,128)} %bitcast.16, f32[2,32]{1,0:T(2,128)} %bitcast.17, bf16[1,2048,896]{2,1,0:T(8,128)(2,1)} %eg_hbm.1, ...), custom_call_target="tpu_custom_call" | custom-call | tf_op jit(solution)/shard_map/tail/pallas_call | solution.py:680
  50.8 1.4 %copy.27 = bf16[32,512]{1,0:T(8,128)(2,1)} copy(bf16[32,512]{1,0:T(8,128)(2,1)} %tail.1) | data formatting | bytes 65536

commit v2 on v1

--- a/solution.py
+++ b/solution.py
@@ -11,60 +11,90 @@
 
 
 def front_kernel(
-    hidden_ref,
-    gains_ref,
-    in_ref,
-    forget_ref,
-    bias_ref,
-    norm_ref,
-    max_ref,
+    hidden_hbm,
+    gains_hbm,
+    in_hbm,
+    forget_hbm,
+    bias_hbm,
+    norm_hbm,
+    max_hbm,
     wq_hbm,
     wk_hbm,
     wv_hbm,
     wo_hbm,
     wm_hbm,
     state_hbm,
-    terms_ref,
+    terms_hbm,
     matrix_hbm,
-    new_norm_ref,
+    new_norm_hbm,
     new_max_ref,
     wq,
     wk,
     wv,
     wo,
     wm,
+    hidden,
+    gains,
+    in_weight,
+    forget_weight,
+    bias,
+    norm,
+    top,
     state,
     numer,
+    terms,
+    new_norms,
+    s_sem,
     w_sem,
     in_sem,
     out_sem,
+    end_sem,
 ):
     tp = lax.axis_index("tp")
     f32, bf16 = jnp.float32, jnp.bfloat16
-    seqs = hidden_ref.shape[0]
+    seqs = hidden.shape[0]
     heads, head = state.shape[1], state.shape[2]
     chunks = in_sem.shape[0]
     step = seqs // chunks
+    smalls = []
+    for i, (src, dst) in enumerate(
+        (
+            (hidden_hbm, hidden),
+            (gains_hbm, gains),
+            (in_hbm, in_weight),
+            (forget_hbm, forget_weight),
+            (bias_hbm, bias),
+            (max_hbm, top),
+            (norm_hbm, norm),
+        )
+    ):
+        smalls.append(pltpu.make_async_copy(src, dst, s_sem.at[i]))
+    for small in smalls[:4]:
+        small.start()
     loads = []
-    for i, (src, dst) in enumerate(((wk_hbm, wk), (wq_hbm, wq), (wv_hbm, wv), (wo_hbm, wo))):
+    for i, (src, dst) in enumerate(((wk_hbm, wk), (wq_hbm, wq), (wv_hbm, wv), (wo_hbm, wo), (wm_hbm, wm))):
         loads.append(pltpu.make_async_copy(src, dst, w_sem.at[i]))
-        loads[i].start()
     fetches = []
     for c in range(chunks):
         rows = pl.ds(c * step, step)
         fetches.append(pltpu.make_async_copy(state_hbm.at[rows], state.at[rows], in_sem.at[c]))
-        fetches[c].start()
-    loads.append(pltpu.make_async_copy(wm_hbm, wm, w_sem.at[4]))
-    loads[4].start()
-
-    start = hidden_ref[...].astype(f32)
+    for load in loads[:3]:
+        load.start()
+    for small in smalls[4:]:
+        small.start()
+    for small in smalls[:4]:
+        small.wait()
+    for fetch in fetches:
+        fetch.start()
+    for load in loads[3:]:
+        load.start()
+
+    start = hidden[...].astype(f32)
     scale = lax.rsqrt(jnp.mean(start * start, axis=1, keepdims=True) + EPS)
-    normed = (start * scale * gains_ref[0:1, :]).astype(bf16)
+    normed = (start * scale * gains[0:1, :]).astype(bf16)
     last = (((1,), (1,)), ((), ()))
-    in_all = lax.dot_general(normed, in_ref[...], last, preferred_element_type=f32)
-    forget_all = lax.dot_general(normed, forget_ref[...], last, preferred_element_type=f32)
-    forget_all = forget_all + bias_ref[...]
-    forget_all = jnp.minimum(forget_all, 0.0) - jnp.log(1.0 + jnp.exp(-jnp.abs(forget_all)))
+    in_all = lax.dot_general(normed, in_weight[...], last, preferred_element_type=f32)
+    forget_all = lax.dot_general(normed, forget_weight[...], last, preferred_element_type=f32)
     column = lax.broadcasted_iota(jnp.int32, in_all.shape, 1)
     here = lax.broadcasted_iota(jnp.int32, (seqs, seqs), 0)
     there = lax.broadcasted_iota(jnp.int32, (seqs, seqs), 1)
@@ -74,20 +104,20 @@
         product = jnp.dot(normed, weight[...], preferred_element_type=f32)
         projected.append(product.astype(bf16).astype(f32))
     keys, query, values = projected
-    pieces = []
-    for h in range(heads):
-        span = slice(h * head, (h + 1) * head)
-        pieces.extend((keys[:, span], query[:, span]))
-    turned = jnp.concatenate(pieces, axis=0).T
+    for small in smalls[4:]:
+        small.wait()
+    forget_all = forget_all + bias[...]
+    forget_all = jnp.minimum(forget_all, 0.0) - jnp.log(1.0 + jnp.exp(-jnp.abs(forget_all)))
     keeps = []
-    adds = []
     bounds = []
+    outers = []
+    turns = []
     for h in range(heads):
         span = slice(h * head, (h + 1) * head)
         mine = column == tp * heads + h
         in_gate = jnp.sum(jnp.where(mine, in_all, 0.0), axis=1, keepdims=True)
         log_forget = jnp.sum(jnp.where(mine, forget_all, 0.0), axis=1, keepdims=True)
-        before = jnp.sum(jnp.where(here == there, max_ref[h : h + 1, :], 0.0), axis=1, keepdims=True)
+        before = jnp.sum(jnp.where(here == there, top[h : h + 1, :], 0.0), axis=1, keepdims=True)
         carried = log_forget + before
         new_max = jnp.maximum(carried, in_gate)
         keep = jnp.exp(carried - new_max)
@@ -95,23 +125,40 @@
         new_max_ref[h : h + 1, :] = jnp.sum(
             jnp.where(here == there, new_max, 0.0), axis=0, keepdims=True
         )
-        new_norm = keep * norm_ref[:, h, :] + write * keys[:, span]
-        new_norm_ref[:, h, :] = new_norm
+        new_norm = keep * norm[:, h, :] + write * keys[:, span]
+        new_norms[:, h, :] = new_norm
         denom = jnp.sum(query[:, span] * new_norm, axis=1, keepdims=True)
         bounds.append(jnp.maximum(jnp.abs(denom), jnp.exp(-new_max)))
         keeps.append(jnp.broadcast_to(keep, (seqs, head)))
-        adds.append(write * values[:, span])
+        added = write * values[:, span]
+        high = added.astype(bf16).astype(f32)
+        middle = (added - high).astype(bf16).astype(f32)
+        low = (added - high - middle).astype(bf16).astype(f32)
+        outers.append(jnp.concatenate([high, middle, low, jnp.zeros_like(low)], axis=0))
+        turned = jnp.concatenate([keys[:, span]] * 3 + [query[:, span]], axis=0).T
+        turns.append((turned, turned.astype(bf16)))
+    norm_store = pltpu.make_async_copy(new_norms, new_norm_hbm, end_sem.at[0])
+    norm_store.start()
+    from_seq = lax.rem(lax.broadcasted_iota(jnp.int32, outers[0].shape, 0), seqs)
     stores = []
     for c in range(chunks):
         fetches[c].wait()
-        for s in range(c * step, (c + 1) * step):
+        for s in range(c * step, (c + 1) * step, 2):
             for h in range(heads):
-                at = 2 * h * seqs + s
-                key_col = turned[:, at : at + 1]
-                query_col = turned[:, at + seqs : at + seqs + 1]
-                new = keeps[h][s : s + 1, :] * state[s, h] + key_col * adds[h][s : s + 1, :]
-                state[s, h] = new
-                numer[h, s : s + 1, :] = jnp.sum(query_col * new, axis=0, keepdims=True)
+                turned, turned_half = turns[h]
+                picked = [jnp.where(from_seq == s + i, outers[h], 0.0).astype(bf16) for i in range(2)]
+                written = jnp.dot(
+                    turned_half, jnp.concatenate(picked, axis=1), preferred_element_type=f32
+                )
+                for i in range(2):
+                    at = 3 * seqs + s + i
+                    query_col = turned[:, at : at + 1]
+                    new = (
+                        keeps[h][s + i : s + i + 1, :] * state[s + i, h]
+                        + written[:, i * head : (i + 1) * head]
+                    )
+                    state[s + i, h] = new
+                    numer[h, s + i : s + i + 1, :] = jnp.sum(query_col * new, axis=0, keepdims=True)
         rows = pl.ds(c * step, step)
         stores.append(pltpu.make_async_copy(state.at[rows], matrix_hbm.at[rows], out_sem.at[c]))
         stores[c].start()
@@ -123,12 +170,14 @@
         mixed.append((jax.nn.sigmoid(gate[:, span]) * (numer[h] / bounds[h])).astype(bf16))
     mixed = jnp.concatenate(mixed, axis=1)
     loads[4].wait()
-    part = terms_ref.shape[2]
-    for t in range(terms_ref.shape[0]):
-        terms_ref[t] = jnp.dot(
+    part = terms.shape[2]
+    for t in range(terms.shape[0]):
+        terms[t] = jnp.dot(
             mixed, wm[:, t * part : (t + 1) * part], preferred_element_type=f32
         ).astype(bf16)
-    for store in stores:
+    terms_store = pltpu.make_async_copy(terms, terms_hbm, end_sem.at[1])
+    terms_store.start()
+    for store in stores + [norm_store, terms_store]:
         store.wait()
 
 
@@ -140,6 +189,15 @@
     chunks = 4
     vmem = pl.BlockSpec(memory_space=pltpu.VMEM)
     hbm = pl.BlockSpec(memory_space=pl.ANY)
+    smalls = (
+        hidden,
+        norm_gains,
+        gate_weights[0].T,
+        gate_weights[1].T,
+        forget_bias.reshape(1, -1),
+        state_norm,
+        state_max.T,
+    )
     terms, matrix, norm, top = pl.pallas_call(
         front_kernel,
         out_shape=(
@@ -148,29 +206,24 @@
             jax.ShapeDtypeStruct(state_norm.shape, f32),
             jax.ShapeDtypeStruct((heads, seqs), f32),
         ),
-        in_specs=[vmem] * 7 + [hbm] * 6,
-        out_specs=(vmem, hbm, vmem, vmem),
+        in_specs=[hbm] * 13,
+        out_specs=(hbm, hbm, hbm, vmem),
         scratch_shapes=[pltpu.VMEM(weight.shape, bf16) for weight in weights]
+        + [pltpu.VMEM(small.shape, small.dtype) for small in smalls]
         + [
             pltpu.VMEM(state_matrix.shape, f32),
             pltpu.VMEM((heads, seqs, head), f32),
+            pltpu.VMEM((tp_count, seqs, width // tp_count), bf16),
+            pltpu.VMEM(state_norm.shape, f32),
+            pltpu.SemaphoreType.DMA((7,)),
             pltpu.SemaphoreType.DMA((5,)),
             pltpu.SemaphoreType.DMA((chunks,)),
             pltpu.SemaphoreType.DMA((chunks,)),
+            pltpu.SemaphoreType.DMA((2,)),
         ],
         compiler_params=pltpu.CompilerParams(vmem_limit_bytes=67043328),
         name="front",
-    )(
-        hidden,
-        norm_gains,
-        gate_weights[0].T,
-        gate_weights[1].T,
-        forget_bias.reshape(1, -1),
-        state_norm,
-        state_max.T,
-        *weights,
-        state_matrix,
-    )
+    )(*smalls, *weights, state_matrix)
     return terms, matrix, norm, top.T
 
 
@@ -207,6 +260,8 @@
     dg,
     du,
     dd,
+    dgt,
+    dut,
     br_recv,
     st_send,
     st_recv,
@@ -232,6 +287,8 @@
     c_recv,
     s_sem,
     w_sem,
+    join_sem,
+    go_sem,
     tp_send,
     tp_recv,
     ep_send,
@@ -245,10 +302,6 @@
     chunk_rows = per * seqs
     chunk_slots = per * capacity
     quarter = chunk_rows // tp_count
-    halves = 2
-    half_chunks = chunks // halves
-    half_slots = half_chunks * chunk_slots
-    half_rows = half_chunks * chunk_rows
     first = pl.multiple_of(tp * part, part)
     f32, bf16 = jnp.float32, jnp.bfloat16
 
@@ -268,15 +321,25 @@
         load.start()
         smalls.append(load)
 
+    gray = [k ^ (k >> 1) for k in range(chunks)]
+    order = [gray[k] * per + i for k in range(chunks) for i in range(per)]
+
+    def partner(p):
+        other = ep
+        bit = 1
+        while bit < ep_count:
+            if order[p] & bit:
+                other = other + bit * (1 - 2 * lax.rem(ep // bit, 2))
+            bit *= 2
+        return other
+
     barrier = pltpu.get_barrier_semaphore()
     for d in range(1, tp_count):
-        pl.semaphore_signal(
-            barrier, inc=1, device_id={"tp": lax.rem(tp + d, tp_count)}, device_id_type=MESH
-        )
-    for d in range(1, ep_count):
-        pl.semaphore_signal(
-            barrier, inc=1, device_id={"ep": lax.rem(ep + d, ep_count)}, device_id_type=MESH
-        )
+        peer = lax.rem(tp + d, tp_count)
+
+        @pl.when(peer != 0)
+        def _(peer=peer):
+            pl.semaphore_signal(barrier, inc=1, device_id={"tp": peer}, device_id_type=MESH)
 
     loads = []
     for i, (src, dst) in enumerate(
@@ -309,18 +372,6 @@
         started.append(copy)
         return copy
 
-    gray = [k ^ (k >> 1) for k in range(chunks)]
-    order = [gray[k] * per + i for k in range(chunks) for i in range(per)]
-
-    def partner(p):
-        other = ep
-        bit = 1
-        while bit < ep_count:
-            if order[p] & bit:
-                other = other + bit * (1 - 2 * lax.rem(ep // bit, 2))
-            bit *= 2
-        return other
-
     def ep_copy(src, dst, p):
         at = ep_next[0]
         ep_next[0] += 1
@@ -386,7 +437,7 @@
     def columns(peer):
         return pl.ds(pl.multiple_of(peer * part, part), part)
 
-    for ref in (st_send, fs_send, mg_send, info_send):
+    for ref in (fs_send, mg_send, info_send):
         ref[...] = jnp.zeros(ref.shape, f32)
     here = lax.broadcasted_iota(jnp.int32, (seqs, seqs), 0)
     there = lax.broadcasted_iota(jnp.int32, (seqs, seqs), 1)
@@ -400,7 +451,18 @@
 
     for load in smalls:
         load.wait()
-    pl.semaphore_wait(barrier, tp_count - 1 + ep_count - 1)
+
+    @pl.when(tp != 0)
+    def _():
+        pl.semaphore_wait(barrier, tp_count - 1)
+        pl.semaphore_signal(join_sem, inc=1, device_id={"tp": 0}, device_id_type=MESH)
+
+    @pl.when(tp == 0)
+    def _():
+        pl.semaphore_wait(join_sem, tp_count - 1)
+        for p in range(1, ep_count):
+            pl.semaphore_signal(barrier, inc=1, device_id={"ep": partner(p)}, device_id_type=MESH)
+
     branch_copies = tp_all(lambda peer: terms.at[peer], br_recv.at[tp])
 
     top = routes.shape[0]
@@ -421,7 +483,6 @@
         share = share + jnp.where(hits[k], scores[k : k + 1, :] / score_sum, 0.0)
     info_send[0, :, 0:seqs] = named * rank
     info_send[1, :, 0:seqs] = share
-    info_copies = [ep_copy(info_send, info_recv.at[p], p) for p in range(1, ep_count)]
 
     start_part = start_in[...].astype(f32)
     gain_one = gains[1:2, :]
@@ -431,57 +492,92 @@
     start_sq = jnp.sum(start_part * start_part, axis=1, keepdims=True)
     start_dot = jnp.sum(start_part * mix_weight, axis=1, keepdims=True)
     branch = terms[tp].astype(f32)
+    loads[0].wait()
+    dgt[...] = dg[...].T
     arrive(branch_copies)
     for d in range(1, tp_count):
         branch = branch + br_recv[from_tp(d)].astype(f32)
     branch = branch.astype(bf16).astype(f32)
     lifted = gain_one * branch
-    sums = (
-        jnp.sum(branch * branch, axis=1, keepdims=True),
-        start_sq,
-        jnp.sum(start_part * lifted, axis=1, keepdims=True),
-        jnp.sum(lifted * lifted, axis=1, keepdims=True),
-        start_dot,
-        jnp.sum(lifted * mix_weight, axis=1, keepdims=True),
+    lanes = st_send.shape[1]
+    lane = lax.broadcasted_iota(jnp.int32, (seqs, lanes), 1)
+    place_of = lax.broadcasted_iota(jnp.int32, (seqs, lanes), 0)
+
+    def pack(values):
+        made = jnp.zeros((seqs, lanes), f32)
+        for i, value in enumerate(values):
+            made = jnp.where(lane == place_of + i * seqs, value, made)
+        return jnp.sum(made, axis=0, keepdims=True)
+
+    def unpack(row, i):
+        return jnp.sum(jnp.where(lane == place_of + i * seqs, row, 0.0), axis=1, keepdims=True)
+
+    packed = pack(
+        (
+            jnp.sum(branch * branch, axis=1, keepdims=True),
+            start_sq,
+            jnp.sum(start_part * lifted, axis=1, keepdims=True),
+            jnp.sum(lifted * lifted, axis=1, keepdims=True),
+            start_dot,
+            jnp.sum(lifted * mix_weight, axis=1, keepdims=True),
+        )
     )
-    for i, value in enumerate(sums):
-        st_send[i : i + 1, 0:seqs] = to_row(value)
+    st_send[...] = packed
     stat_copies = tp_all(lambda peer: st_send, st_recv.at[tp])
-    packed = st_send[...]
+
+    @pl.when(tp == 0)
+    def _():
+        pl.semaphore_wait(barrier, ep_count - 1)
+        for t in range(1, tp_count):
+            pl.semaphore_signal(go_sem, inc=1, device_id={"tp": t}, device_id_type=MESH)
+
+    @pl.when(tp != 0)
+    def _():
+        pl.semaphore_wait(go_sem, 1)
+
+    info_copies = [ep_copy(info_send, info_recv.at[p], p) for p in range(1, ep_count)]
+    loads[1].wait()
+    dut[...] = du[...].T
     arrive(stat_copies)
     for d in range(1, tp_count):
         packed = packed + st_recv[from_tp(d)]
     branch_sq, start_sq, cross_sum, lifted_sq, start_dot, lifted_dot = (
-        packed[i : i + 1, 0:seqs] for i in range(6)
+        unpack(packed, i) for i in range(6)
     )
     branch_scale = lax.rsqrt(branch_sq / width + EPS)
     resid_sq = start_sq + 2.0 * branch_scale * cross_sum + branch_scale * branch_scale * lifted_sq
     gate_dot = start_dot + branch_scale * lifted_dot
     scale_two = lax.rsqrt(resid_sq / width + EPS)
-    mg_send[0:1, 0:seqs] = jax.nn.sigmoid(scale_two * gate_dot)
-    residual_f = start_part + lifted * to_column(branch_scale)
+    residual_f = start_part + lifted * branch_scale
     residual = residual_f.astype(bf16).astype(f32)
-    rows_in[0] = (residual_f * to_column(scale_two) * gain_two).astype(bf16)
-    row_copies = [ep_copy(rows_in.at[0], rows_in.at[p], p) for p in range(1, ep_count)]
+    rows_in[0] = (residual_f * scale_two * gain_two).astype(bf16)
+    row_copies = [None] * ep_count
+    for p in range(1, ep_count):
+        row_copies[p] = ep_copy(rows_in.at[0], rows_in.at[p], p)
+    mix_gate = jax.nn.sigmoid(scale_two * gate_dot)
+    mg_send[0:1, 0:seqs] = to_row(mix_gate)
     mg_copies = [ep_copy(mg_send, mg_recv.at[p], p) for p in range(1, ep_count)]
-
     mine = lax.broadcasted_iota(jnp.int32, (experts, seqs), 0) == ep
     wanted = (lax.broadcasted_iota(jnp.int32, (capacity, seqs), 0) + 1).astype(f32)
+    wide_row = lax.broadcasted_iota(jnp.int32, (seqs, chunk_rows), 0)
+    wide_column = lax.broadcasted_iota(jnp.int32, (seqs, chunk_rows), 1)
+    arrive(info_copies)
     placings = []
     shares = []
-
-    def place(p):
-        if p == 0:
-            codes, portion = info_send[0], info_send[1]
-        else:
-            info_copies[p - 1].wait_recv()
-            codes, portion = info_recv[p, 0], info_recv[p, 1]
-        code = jnp.sum(jnp.where(mine, codes[:, 0:seqs], 0.0), axis=0, keepdims=True)
-        placings.append(jnp.where(code == wanted, 1.0, 0.0).astype(bf16))
-        shares.append(jnp.sum(jnp.where(mine, portion[:, 0:seqs], 0.0), axis=0, keepdims=True))
-
-    def slots_of(p):
-        return pl.ds(p * capacity, capacity)
+    for k in range(chunks):
+        blocks = []
+        for q in range(per):
+            p = k * per + q
+            if p == 0:
+                codes, portion = info_send[0], info_send[1]
+            else:
+                codes, portion = info_recv[p, 0], info_recv[p, 1]
+            code = jnp.sum(jnp.where(mine, codes[:, 0:seqs], 0.0), axis=0, keepdims=True)
+            one = jnp.where(code == wanted, 1.0, 0.0).astype(bf16)
+            moved = jnp.where(wide_row + q * seqs == wide_column, 1.0, 0.0).astype(bf16)
+            blocks.append(jnp.dot(one, moved, preferred_element_type=f32).astype(bf16))
+            shares.append(to_column(jnp.sum(jnp.where(mine, portion[:, 0:seqs], 0.0), axis=0, keepdims=True)))
+        placings.append(jnp.concatenate(blocks, axis=0))
 
     def xin_at(k):
         return lambda i: xin.at[i, pl.ds(k * chunk_slots, chunk_slots)]
@@ -495,29 +591,21 @@
     def hid_at(k):
         return lambda i: hid.at[k, i]
 
-    def half_of(ref, h):
-        return lambda i: ref.at[i, pl.ds(h * half_slots, half_slots)]
-
-    last = (((1,), (1,)), ((), ()))
     xin_copies = []
     pre_copies = []
     hid_copies = []
 
     def chunk_in(k):
         for p in range(k * per, (k + 1) * per):
-            place(p)
             if p > 0:
-                row_copies[p - 1].wait_recv()
-            xin[tp, slots_of(p)] = jnp.dot(
-                placings[p], rows_in[p], preferred_element_type=f32
-            ).astype(bf16)
+                row_copies[p].wait_recv()
+        rows = rows_in[k * per : (k + 1) * per].reshape(chunk_rows, part)
+        xin[tp, k * chunk_slots : (k + 1) * chunk_slots] = jnp.dot(
+            placings[k], rows, preferred_element_type=f32
+        ).astype(bf16)
         xin_copies.append(gather_start(xin_at(k)))
-        if k == 0:
-            loads[0].wait()
-            loads[1].wait()
-        rows = rows_in[k * per : (k + 1) * per].reshape(chunk_rows, part)
-        for i, weight in enumerate((dg, du)):
-            made = lax.dot_general(rows, weight[...], last, preferred_element_type=f32).astype(bf16)
+        for i, weight in enumerate((dgt, dut)):
+            made = jnp.dot(rows, weight[...], preferred_element_type=f32).astype(bf16)
             for t in range(tp_count):
                 pre_send[k, t, i] = made[t * quarter : (t + 1) * quarter]
         pre_copies.append(scatter_pair(pre_at(k), of(pre_one, k)))
@@ -543,18 +631,20 @@
             made = jnp.dot(xin[source], weight[columns(source), :], preferred_element_type=f32)
             sums_of[i] = made if sums_of[i] is None else sums_of[i] + made
 
-    for k in range(chunks):
+    chunk_in(0)
+    pre_cross(0)
+    for k in range(1, chunks):
         chunk_in(k)
-        if k >= 1:
+        if k >= 2:
             pre_cross(k - 1)
-        if k >= 2:
-            xin_relay(k - 2)
-    if chunks >= 2:
-        xin_relay(chunks - 2)
+    arrive(mg_copies)
+    gates = [mix_gate] + [to_column(mg_recv[p, 0:1, 0:seqs]) for p in range(1, ep_count)]
     loads[2].wait()
     loads[3].wait()
     expert_in(tp)
     pre_cross(chunks - 1)
+    for k in range(chunks - 1):
+        xin_relay(k)
     pre_done(0)
     for k in range(chunks):
         xin_copies[k][groups - 1].wait_recv()
@@ -571,70 +661,76 @@
     hidden_units = (jax.nn.silu(sums_of[0]) * sums_of[1]).astype(bf16)
 
     loads[4].wait()
-    eo_copies = [None] * halves
-    turn = list(range(halves))[::-1]
-
-    def expert_down(h, t):
-        eo_send[t, h * half_slots : (h + 1) * half_slots] = jnp.dot(
-            hidden_units[h * half_slots : (h + 1) * half_slots],
-            ed[:, columns(t)],
-            preferred_element_type=f32,
-        ).astype(bf16)
-
-    for h in turn:
-        for j in range(groups):
-            expert_down(h, j * 2 + 1 - parity)
-        eo_copies[h] = scatter_pair(half_of(eo_send, h), half_of(eo_one, h))
+    eo_copies = [None] * chunks
+    turn = list(range(chunks))[::-1]
+
+    def piece_of(ref, k):
+        return lambda i: ref.at[i, pl.ds(k * chunk_slots, chunk_slots)]
+
+    def expert_down(t):
+        eo_send[t] = jnp.dot(hidden_units, ed[:, columns(t)], preferred_element_type=f32).astype(bf16)
+
     for k in range(3, chunks):
         pre_done(k)
-    for k in range(chunks - 1):
+    for j in range(groups):
+        expert_down(j * 2 + 1 - parity)
+    for k in turn:
+        eo_copies[k] = scatter_pair(piece_of(eo_send, k), piece_of(eo_one, k))
+    for j in range(groups):
+        expert_down(j * 2 + parity)
+    hid_relay(0)
+    for k in turn:
+        scatter_cross(
+            piece_of(eo_send, k), piece_of(eo_one, k), piece_of(eo_mid, k), piece_of(eo_two, k), eo_copies[k]
+        )
+    for k in range(1, chunks):
         hid_relay(k)
-    for h in turn:
-        for j in range(groups):
-            expert_down(h, j * 2 + parity)
-        scatter_cross(
-            half_of(eo_send, h), half_of(eo_one, h), half_of(eo_mid, h), half_of(eo_two, h), eo_copies[h]
-        )
-    hid_relay(chunks - 1)
     loads[5].wait()
+    units = hid.shape[3]
+    for k in range(chunks):
+        arrive(hid_copies[k][groups - 1 :])
+    dense_out[...] = jnp.dot(
+        hid[...].reshape(ep_count * seqs, units), dd[...], preferred_element_type=f32
+    )
+    for p in range(ep_count):
+        rows = slice(p * seqs, (p + 1) * seqs)
+        dense_out[rows] = gates[p] * dense_out[rows]
+    relayed = range(chunks // 2, chunks)
     c_copies = {}
-    mixed = None
-    for h in turn:
-        for k in range(h * half_chunks, (h + 1) * half_chunks):
-            arrive(hid_copies[k][groups - 1 :])
-        units = hid.shape[3]
-        dense_out[h * half_rows : (h + 1) * half_rows] = jnp.dot(
-            hid[h * half_chunks : (h + 1) * half_chunks].reshape(half_rows, units),
-            dd[...],
-            preferred_element_type=f32,
-        )
+    parts = {}
+    near = {}
     first_dims = (((0,), (0,)), ((), ()))
-    for h in turn:
-        total = scatter_sum(half_of(eo_send, h), half_of(eo_one, h), half_of(eo_two, h), eo_copies[h])
+
+    def c_cross(k):
+        for p in range(k * per, (k + 1) * per, 2):
+            near[p].wait_recv()
+            c_send[p] = (parts[p] + c_recv[p + 1].astype(f32)).astype(bf16)
+            c_copies[p] = ep_copy(c_send.at[p], c_recv.at[p], p)
+
+    for k in turn:
+        total = scatter_sum(piece_of(eo_send, k), piece_of(eo_one, k), piece_of(eo_two, k), eo_copies[k])
         total = total.astype(bf16)
-        for q in list(range(half_chunks * per))[::-1]:
-            p = h * half_chunks * per + q
-            picked = lax.dot_general(
-                placings[p],
-                total[q * capacity : (q + 1) * capacity],
-                first_dims,
-                preferred_element_type=f32,
+        picked = lax.dot_general(placings[k], total, first_dims, preferred_element_type=f32)
+        for q in list(range(per))[::-1]:
+            p = k * per + q
+            combined = (
+                dense_out[p * seqs : (p + 1) * seqs] + shares[p] * picked[q * seqs : (q + 1) * seqs]
             )
             if p == 0:
-                gate = mg_send[0:1, 0:seqs]
-            else:
-                mg_copies[p - 1].wait_recv()
-                gate = mg_recv[p, 0:1, 0:seqs]
-            combined = (
-                to_column(gate) * dense_out[p * seqs : (p + 1) * seqs] + to_column(shares[p]) * picked
-            )
-            if p == 0:
-                mixed = combined
+                parts[p] = combined
+            elif k in relayed and p % 2 == 0:
+                parts[p] = combined
             else:
                 c_send[p] = combined.astype(bf16)
-                c_copies[p] = ep_copy(c_send.at[p], c_recv.at[p], p)
-    ffn = mixed
-    for p in range(1, ep_count):
+                if k in relayed:
+                    near[p - 1] = ep_copy(c_send.at[p], c_recv.at[p], 1)
+                else:
+                    c_copies[p] = ep_copy(c_send.at[p], c_recv.at[p], p)
+        if k == 0:
+            for late in reversed(relayed):
+                c_cross(late)
+    ffn = parts[0]
+    for p in sorted(c_copies):
         c_copies[p].wait_recv()
         ffn = ffn + c_recv[p].astype(f32)
     fs_send[0:1, 0:seqs] = to_row(jnp.sum(ffn * ffn, axis=1, keepdims=True))
@@ -674,8 +770,9 @@
     vmem = pl.BlockSpec(memory_space=pltpu.VMEM)
     hbm = pl.BlockSpec(memory_space=pl.ANY)
     slots = ep_count * capacity
-    tp_copies = 3 * (tp_count - 1) + (3 * chunks + 2) * (2 * groups - 1)
+    tp_copies = 3 * (tp_count - 1) + 4 * chunks * (2 * groups - 1)
     ep_copies = 4 * (ep_count - 1)
+    sums = -(-6 * seqs // 128) * 128
     piece = pltpu.VMEM((chunks, groups, 2, quarter, dense_units), bf16)
     return pl.pallas_call(
         functools.partial(tail_kernel, tp_count, ep_count, capacity, chunks),
@@ -695,9 +792,11 @@
             pltpu.VMEM(dense_gate.shape, bf16),
             pltpu.VMEM(dense_up.shape, bf16),
             pltpu.VMEM(dense_down.shape, bf16),
+            pltpu.VMEM(dense_gate.shape[::-1], bf16),
+            pltpu.VMEM(dense_up.shape[::-1], bf16),
             pltpu.VMEM((tp_count, seqs, part), bf16),
-            pltpu.VMEM((8, lanes), f32),
-            pltpu.VMEM((tp_count, 8, lanes), f32),
+            pltpu.VMEM((1, sums), f32),
+            pltpu.VMEM((tp_count, 1, sums), f32),
             pltpu.VMEM((1, lanes), f32),
             pltpu.VMEM((tp_count, 1, lanes), f32),
             pltpu.VMEM((2, experts, lanes), f32),
@@ -720,6 +819,8 @@
             pltpu.VMEM((ep_count, seqs, part), bf16),
             pltpu.SemaphoreType.DMA((6,)),
             pltpu.SemaphoreType.DMA((6,)),
+            pltpu.SemaphoreType.REGULAR,
+            pltpu.SemaphoreType.REGULAR,
             pltpu.SemaphoreType.DMA((tp_copies,)),
             pltpu.SemaphoreType.DMA((tp_copies,)),
             pltpu.SemaphoreType.DMA((ep_copies,)),

time: 52.4 us -> 50.3 us (0.960)
  Pallas kernels: 50.2 us -> 48.1 us
    pallas_call x1, Pallas kernels: 7.98 us -> 6.8 us  [front(): pl.pallas_call(front_kernel, out_shape=(jax.ShapeDtypeStruct((tp_count, s...]
    pallas_call x1, Pallas kernels: 42.2 us -> 41.3 us  [tail(): pl.pallas_call(functools.partial(tail_kernel, tp_count, ep_count, capacit...]
where the time goes in v2:
time: 50.3 us; the launch traced here: 50.2 us
  Pallas kernels  48.1 us (96%)
  local copies, waits for them, and re-layouts  1.38 us (3%)
  between operations  0.65 us (1%)
    pallas_call x1, Pallas kernels, tail(): pl.pallas_call(functools.partial(tail_kernel, tp_count, ep_count, capacit...  41.3 us
    pallas_call x1, Pallas kernels, front(): pl.pallas_call(front_kernel, out_shape=(jax.ShapeDtypeStruct((tp_count, s...  6.8 us
    unnamed x1, local copies, waits for them, and re-layouts  1.38 us

profile of v2, /device:TPU:0, one launch (start us, length us, event | category | flops | bytes accessed | tf_op | source)
XLA Modules:
  0.0 50.2 jit_solution(6784252465445341331)
XLA Ops:
  0.6 6.8 %front.1 = (bf16[4,32,512]{2,1,0:T(8,128)(2,1)}, f32[32,2,128,128]{3,2,1,0:T(8,128)}, f32[32,2,128]{2,1,0:T(2,128)}, f32[2,32]{1,0:T(2,128)}) custom-call(bf16[32,2048]{1,0:T(8,128)(2,1)} %hidden_hbm.3, f32[4,2048]{1,0:T(4,128)} %gains_hbm.3, bf16[8,2048]{1,0:T(8,128)(2,1)} %bitcast.12, bf16[8,2048]{1,0:T(8,128)(2,1)} %bitcast.13, f32[1,8]{1,0:T(1,128)} %bitcast.18, ...), custom_call_target="tpu_custom_call" | custom-call | tf_op jit(solution)/shard_map/front/pallas_call | solution.py:201
  7.4 41.3 %tail.1 = bf16[32,512]{1,0:T(8,128)(2,1)} custom-call(bf16[4,32,512]{2,1,0:T(8,128)(2,1)} %get-tuple-element.8.terms_hbm, bf16[32,2048]{1,0:T(8,128)(2,1)} %hidden_hbm.3, f32[4,2048]{1,0:T(4,128)} %gains_hbm.3, f32[1,2048]{1,0:T(1,128)} %bitcast.14, s32[2,32]{1,0:T(2,128)} %bitcast.16, f32[2,32]{1,0:T(2,128)} %bitcast.17, bf16[1,2048,896]{2,1,0:T(8,128)(2,1)} %eg_hbm.1, ...), custom_call_target="tpu_custom_call" | custom-call | tf_op jit(solution)/shard_map/tail/pallas_call | solution.py:777
  48.8 1.4 %copy.27 = bf16[32,512]{1,0:T(8,128)(2,1)} copy(bf16[32,512]{1,0:T(8,128)(2,1)} %tail.1) | data formatting | bytes 65536

commit v3 on v2

--- a/solution.py
+++ b/solution.py
@@ -321,14 +321,11 @@
         load.start()
         smalls.append(load)
 
-    gray = [k ^ (k >> 1) for k in range(chunks)]
-    order = [gray[k] * per + i for k in range(chunks) for i in range(per)]
-
     def partner(p):
         other = ep
         bit = 1
         while bit < ep_count:
-            if order[p] & bit:
+            if p & bit:
                 other = other + bit * (1 - 2 * lax.rem(ep // bit, 2))
             bit *= 2
         return other
@@ -410,17 +407,21 @@
             made[d - 1].wait_recv()
             made.append(tp_copy(at(behind(d)), at(behind(d)), pair))
 
-    def scatter_pair(at, one):
-        return [tp_copy(at(j * 2 + 1 - parity), one(j), pair) for j in range(groups)]
+    def other(d):
+        return lax.rem(group + d, groups)
+
+    def scatter_pair(at, one, d):
+        return tp_copy(at(other(d) * 2 + 1 - parity), one(other(d)), pair)
 
     def scatter_cross(at, one, mid, two, made):
-        arrive(made)
         for d in range(1, groups):
-            j = lax.rem(group + d, groups)
+            j = other(d)
+            made[d].wait_recv()
             mid(j)[...] = (at(ahead(d))[...].astype(f32) + one(j)[...].astype(f32)).astype(bf16)
             made.append(tp_copy(mid(j), two(group), ahead(d)))
 
     def scatter_sum(at, one, two, made):
+        made[0].wait_recv()
         total = at(tp)[...].astype(f32) + one(group)[...].astype(f32)
         for d in range(1, groups):
             made[groups + d - 1].wait_recv()
@@ -552,7 +553,7 @@
     residual = residual_f.astype(bf16).astype(f32)
     rows_in[0] = (residual_f * scale_two * gain_two).astype(bf16)
     row_copies = [None] * ep_count
-    for p in range(1, ep_count):
+    for p in list(range(1, ep_count)):
         row_copies[p] = ep_copy(rows_in.at[0], rows_in.at[p], p)
     mix_gate = jax.nn.sigmoid(scale_two * gate_dot)
     mg_send[0:1, 0:seqs] = to_row(mix_gate)
@@ -608,7 +609,9 @@
             made = jnp.dot(rows, weight[...], preferred_element_type=f32).astype(bf16)
             for t in range(tp_count):
                 pre_send[k, t, i] = made[t * quarter : (t + 1) * quarter]
-        pre_copies.append(scatter_pair(pre_at(k), of(pre_one, k)))
+        far_first = list(range(1, groups)) + [0]
+        made = {d: scatter_pair(pre_at(k), of(pre_one, k), d) for d in far_first}
+        pre_copies.append([made[d] for d in range(groups)])
 
     def pre_cross(k):
         scatter_cross(pre_at(k), of(pre_one, k), of(pre_mid, k), of(pre_two, k), pre_copies[k])
@@ -661,7 +664,6 @@
     hidden_units = (jax.nn.silu(sums_of[0]) * sums_of[1]).astype(bf16)
 
     loads[4].wait()
-    eo_copies = [None] * chunks
     turn = list(range(chunks))[::-1]
 
     def piece_of(ref, k):
@@ -670,20 +672,26 @@
     def expert_down(t):
         eo_send[t] = jnp.dot(hidden_units, ed[:, columns(t)], preferred_element_type=f32).astype(bf16)
 
+    eo_copies = [[None] * groups for k in range(chunks)]
+
+    def expert_pair(d):
+        expert_down(other(d) * 2 + 1 - parity)
+        for k in turn:
+            eo_copies[k][d] = scatter_pair(piece_of(eo_send, k), piece_of(eo_one, k), d)
+
+    for d in range(1, groups):
+        expert_pair(d)
     for k in range(3, chunks):
         pre_done(k)
-    for j in range(groups):
-        expert_down(j * 2 + 1 - parity)
-    for k in turn:
-        eo_copies[k] = scatter_pair(piece_of(eo_send, k), piece_of(eo_one, k))
-    for j in range(groups):
-        expert_down(j * 2 + parity)
-    hid_relay(0)
+    for d in range(1, groups):
+        expert_down(ahead(d))
+    expert_pair(0)
     for k in turn:
         scatter_cross(
             piece_of(eo_send, k), piece_of(eo_one, k), piece_of(eo_mid, k), piece_of(eo_two, k), eo_copies[k]
         )
-    for k in range(1, chunks):
+    expert_down(tp)
+    for k in range(chunks):
         hid_relay(k)
     loads[5].wait()
     units = hid.shape[3]
@@ -695,7 +703,7 @@
     for p in range(ep_count):
         rows = slice(p * seqs, (p + 1) * seqs)
         dense_out[rows] = gates[p] * dense_out[rows]
-    relayed = range(chunks // 2, chunks)
+    relayed = range(chunks // 2, chunks // 2 + 1)
     c_copies = {}
     parts = {}
     near = {}

time: 50.3 us -> 48.7 us (0.968)
  Pallas kernels: 48.1 us -> 46.5 us
    pallas_call x1, Pallas kernels: 41.3 us -> 39.7 us  [tail(): pl.pallas_call(functools.partial(tail_kernel, tp_count, ep_count, capacit...]
where the time goes in v3:
time: 48.7 us; the launch traced here: 48.6 us
  Pallas kernels  46.5 us (95%)
  local copies, waits for them, and re-layouts  1.38 us (3%)
  between operations  0.65 us (1%)
    pallas_call x1, Pallas kernels, tail(): pl.pallas_call(functools.partial(tail_kernel, tp_count, ep_count, capacit...  39.7 us
    pallas_call x1, Pallas kernels, front(): pl.pallas_call(front_kernel, out_shape=(jax.ShapeDtypeStruct((tp_count, s...  6.8 us
    unnamed x1, local copies, waits for them, and re-layouts  1.38 us

profile of v3, /device:TPU:0, one launch (start us, length us, event | category | flops | bytes accessed | tf_op | source)
XLA Modules:
  0.0 48.6 jit_solution(15980011456637851323)
XLA Ops:
  0.6 6.8 %front.1 = (bf16[4,32,512]{2,1,0:T(8,128)(2,1)}, f32[32,2,128,128]{3,2,1,0:T(8,128)}, f32[32,2,128]{2,1,0:T(2,128)}, f32[2,32]{1,0:T(2,128)}) custom-call(bf16[32,2048]{1,0:T(8,128)(2,1)} %hidden_hbm.3, f32[4,2048]{1,0:T(4,128)} %gains_hbm.3, bf16[8,2048]{1,0:T(8,128)(2,1)} %bitcast.12, bf16[8,2048]{1,0:T(8,128)(2,1)} %bitcast.13, f32[1,8]{1,0:T(1,128)} %bitcast.18, ...), custom_call_target="tpu_custom_call" | custom-call | tf_op jit(solution)/shard_map/front/pallas_call | solution.py:201
  7.4 39.7 %tail.1 = bf16[32,512]{1,0:T(8,128)(2,1)} custom-call(bf16[4,32,512]{2,1,0:T(8,128)(2,1)} %get-tuple-element.8.terms_hbm, bf16[32,2048]{1,0:T(8,128)(2,1)} %hidden_hbm.3, f32[4,2048]{1,0:T(4,128)} %gains_hbm.3, f32[1,2048]{1,0:T(1,128)} %bitcast.14, s32[2,32]{1,0:T(2,128)} %bitcast.16, f32[2,32]{1,0:T(2,128)} %bitcast.17, bf16[1,2048,896]{2,1,0:T(8,128)(2,1)} %eg_hbm.1, ...), custom_call_target="tpu_custom_call" | custom-call | tf_op jit(solution)/shard_map/tail/pallas_call | solution.py:785
  47.2 1.4 %copy.27 = bf16[32,512]{1,0:T(8,128)(2,1)} copy(bf16[32,512]{1,0:T(8,128)(2,1)} %tail.1) | data formatting | bytes 65536

commit v4 on v3

--- a/solution.py
+++ b/solution.py
@@ -450,8 +450,6 @@
     def to_column(row):
         return jnp.sum(jnp.where(diagonal, row, 0.0), axis=1, keepdims=True)
 
-    for load in smalls:
-        load.wait()
 
     @pl.when(tp != 0)
     def _():
@@ -464,10 +462,12 @@
         for p in range(1, ep_count):
             pl.semaphore_signal(barrier, inc=1, device_id={"ep": partner(p)}, device_id_type=MESH)
 
+    for load in smalls:
+        load.wait()
     branch_copies = tp_all(lambda peer: terms.at[peer], br_recv.at[tp])
 
     top = routes.shape[0]
-    experts = info_send.shape[1]
+    experts = info_send.shape[0]
     name = lax.broadcasted_iota(jnp.int32, (experts, seqs), 0)
     hits = [routes[k : k + 1, :] == name for k in range(top)]
     named = hits[0]
@@ -482,8 +482,7 @@
     share = jnp.zeros((experts, seqs), f32)
     for k in range(top):
         share = share + jnp.where(hits[k], scores[k : k + 1, :] / score_sum, 0.0)
-    info_send[0, :, 0:seqs] = named * rank
-    info_send[1, :, 0:seqs] = share
+    info_send[:, 0 : 2 * seqs] = jnp.concatenate([named * rank, share], axis=1)
 
     start_part = start_in[...].astype(f32)
     gain_one = gains[1:2, :]
@@ -558,7 +557,9 @@
     mix_gate = jax.nn.sigmoid(scale_two * gate_dot)
     mg_send[0:1, 0:seqs] = to_row(mix_gate)
     mg_copies = [ep_copy(mg_send, mg_recv.at[p], p) for p in range(1, ep_count)]
-    mine = lax.broadcasted_iota(jnp.int32, (experts, seqs), 0) == ep
+    mine = lax.broadcasted_iota(jnp.int32, info_send.shape, 0) == ep
+    info_lane = lax.broadcasted_iota(jnp.int32, (seqs, info_send.shape[1]), 1)
+    info_seq = lax.broadcasted_iota(jnp.int32, (seqs, info_send.shape[1]), 0)
     wanted = (lax.broadcasted_iota(jnp.int32, (capacity, seqs), 0) + 1).astype(f32)
     wide_row = lax.broadcasted_iota(jnp.int32, (seqs, chunk_rows), 0)
     wide_column = lax.broadcasted_iota(jnp.int32, (seqs, chunk_rows), 1)
@@ -569,15 +570,14 @@
         blocks = []
         for q in range(per):
             p = k * per + q
-            if p == 0:
-                codes, portion = info_send[0], info_send[1]
-            else:
-                codes, portion = info_recv[p, 0], info_recv[p, 1]
-            code = jnp.sum(jnp.where(mine, codes[:, 0:seqs], 0.0), axis=0, keepdims=True)
-            one = jnp.where(code == wanted, 1.0, 0.0).astype(bf16)
+            info = info_send[...] if p == 0 else info_recv[p]
+            info = jnp.sum(jnp.where(mine, info, 0.0), axis=0, keepdims=True)
+            one = jnp.where(info[:, 0:seqs] == wanted, 1.0, 0.0).astype(bf16)
             moved = jnp.where(wide_row + q * seqs == wide_column, 1.0, 0.0).astype(bf16)
             blocks.append(jnp.dot(one, moved, preferred_element_type=f32).astype(bf16))
-            shares.append(to_column(jnp.sum(jnp.where(mine, portion[:, 0:seqs], 0.0), axis=0, keepdims=True)))
+            shares.append(
+                jnp.sum(jnp.where(info_lane == info_seq + seqs, info, 0.0), axis=1, keepdims=True)
+            )
         placings.append(jnp.concatenate(blocks, axis=0))
 
     def xin_at(k):
@@ -774,6 +774,7 @@
     quarter = rows_all // chunks // tp_count
     groups = tp_count // 2
     lanes = -(-seqs // 128) * 128
+    pairs = -(-2 * seqs // 128) * 128
     f32, bf16 = jnp.float32, jnp.bfloat16
     vmem = pl.BlockSpec(memory_space=pltpu.VMEM)
     hbm = pl.BlockSpec(memory_space=pl.ANY)
@@ -807,8 +808,8 @@
             pltpu.VMEM((tp_count, 1, sums), f32),
             pltpu.VMEM((1, lanes), f32),
             pltpu.VMEM((tp_count, 1, lanes), f32),
-            pltpu.VMEM((2, experts, lanes), f32),
-            pltpu.VMEM((ep_count, 2, experts, lanes), f32),
+            pltpu.VMEM((experts, pairs), f32),
+            pltpu.VMEM((ep_count, experts, pairs), f32),
             pltpu.VMEM((1, lanes), f32),
             pltpu.VMEM((ep_count, 1, lanes), f32),
             pltpu.VMEM((ep_count, seqs, part), bf16),

time: 48.7 us -> 48.3 us (level)
  no operation moved by 1% of the time
where the time goes in v4:
time: 48.3 us; the launch traced here: 48.2 us
  Pallas kernels  46.1 us (95%)
  local copies, waits for them, and re-layouts  1.38 us (3%)
  between operations  0.65 us (1%)
    pallas_call x1, Pallas kernels, tail(): pl.pallas_call(functools.partial(tail_kernel, tp_count, ep_count, capacit...  39.3 us
    pallas_call x1, Pallas kernels, front(): pl.pallas_call(front_kernel, out_shape=(jax.ShapeDtypeStruct((tp_count, s...  6.8 us
    unnamed x1, local copies, waits for them, and re-layouts  1.38 us

profile of v4, /device:TPU:0, one launch (start us, length us, event | category | flops | bytes accessed | tf_op | source)
XLA Modules:
  0.0 48.2 jit_solution(9562603508502847002)
XLA Ops:
  0.6 6.8 %front.1 = (bf16[4,32,512]{2,1,0:T(8,128)(2,1)}, f32[32,2,128,128]{3,2,1,0:T(8,128)}, f32[32,2,128]{2,1,0:T(2,128)}, f32[2,32]{1,0:T(2,128)}) custom-call(bf16[32,2048]{1,0:T(8,128)(2,1)} %hidden_hbm.3, f32[4,2048]{1,0:T(4,128)} %gains_hbm.3, bf16[8,2048]{1,0:T(8,128)(2,1)} %bitcast.12, bf16[8,2048]{1,0:T(8,128)(2,1)} %bitcast.13, f32[1,8]{1,0:T(1,128)} %bitcast.18, ...), custom_call_target="tpu_custom_call" | custom-call | tf_op jit(solution)/shard_map/front/pallas_call | solution.py:201
  7.4 39.3 %tail.1 = bf16[32,512]{1,0:T(8,128)(2,1)} custom-call(bf16[4,32,512]{2,1,0:T(8,128)(2,1)} %get-tuple-element.8.terms_hbm, bf16[32,2048]{1,0:T(8,128)(2,1)} %hidden_hbm.3, f32[4,2048]{1,0:T(4,128)} %gains_hbm.3, f32[1,2048]{1,0:T(1,128)} %bitcast.14, s32[2,32]{1,0:T(2,128)} %bitcast.16, f32[2,32]{1,0:T(2,128)} %bitcast.17, bf16[1,2048,896]{2,1,0:T(8,128)(2,1)} %eg_hbm.1, ...), custom_call_target="tpu_custom_call" | custom-call | tf_op jit(solution)/shard_map/tail/pallas_call | solution.py:786
  46.8 1.4 %copy.27 = bf16[32,512]{1,0:T(8,128)(2,1)} copy(bf16[32,512]{1,0:T(8,128)(2,1)} %tail.1) | data formatting | bytes 65536
